TPU v7x, 256 devices: a whole 4x4x8 slice. The times are simulated.
256 devices in a mesh: sp: 64 (over z, y, core), tp: 4 (over x).
Axes of the slice: x: 4, y: 4, z: 8, core: 2. Of those that a mesh axis runs over, the one named last changes fastest.
Arguments:
- queries: bfloat16 [49152, 1536], P('sp', 'tp'), may hold values from -130 to 130, as said below
- keys: bfloat16 [49152, 512], P('sp', 'tp'), may hold values from -6 to 6
- values: bfloat16 [49152, 512], P('sp', 'tp'), may hold values from -6 to 6
- residual: bfloat16 [49152, 2048], P(('sp', 'tp')), may hold values from -6 to 6
- sinks: float32 [12], P('tp'), may hold values from 2 to 6
- out_weight: bfloat16 [1536, 2048], P('tp'), may hold values from -0.15625 to 0.15625
- up_weight: bfloat16 [2048, 8192], P('sp', 'tp'), may hold values from -0.125 to 0.125
- down_weight: bfloat16 [8192, 2048], P('tp', 'sp'), may hold values from -0.0625 to 0.0625
- gains: float32 [2, 2048], replicated, may hold values from 0.1 to 1.9
- biases: float32 [2, 2048], replicated, may hold values from -3 to 3
Outputs:
- layer_out: bfloat16 [49152, 2048], P(('sp', 'tp'))
Inputs may be any that keep to these rules, and one draw needn't show every extreme that they name: `queries`: entries of order one, with some rows far larger in some draws.
All inputs are finite; a program needn't handle non-finite values.
Results may differ from a plain program's by a relative error of at most 0.0095.
Values may be sent and summed in bfloat16 or wider, within the bound.
No kernel may reach another device: no remote copies, remote signals or barrier semaphores. Data moves between devices by JAX's collectives and lax.ppermute only.
A program may use at most 128 MiB of HBM per device.

v0:
```python
import functools

import jax
import jax.numpy as jnp
from jax import lax
from jax.experimental import pallas as pl
from jax.experimental.pallas import tpu as pltpu
from jax.sharding import PartitionSpec as P


HEADS = 12
HEAD = 128
WINDOW = 128
Y, Z = 4, 8
NEAR = 1792

deep_alpha = 1.6817928
norm_eps = 1e-05
neg_big = -1e30


VMEM = pl.BlockSpec(memory_space=pltpu.VMEM)
SMEM = pl.BlockSpec(memory_space=pltpu.SMEM)
HBM = pl.BlockSpec(memory_space=pltpu.HBM)


def call(body, outs, args, specs, flops, mib, scratch=()):
    return pl.pallas_call(
        body,
        out_shape=outs,
        in_specs=specs,
        out_specs=jax.tree.map(lambda _: VMEM, outs),
        scratch_shapes=list(scratch),
        compiler_params=pltpu.CompilerParams(vmem_limit_bytes=mib * 2**20),
        cost_estimate=pl.CostEstimate(flops=flops, transcendentals=0, bytes_accessed=0),
    )(*args)


def sp_route(to):
    pairs = []
    for i in range(Z * Y * 2):
        z, y, c = to(i // (2 * Y), i // 2 % Y, i % 2)
        pairs.append((i, z % Z * 2 * Y + y % Y * 2 + c))
    return pairs


def z_first(block, flip=0):
    def to(z, y, c):
        return (z ^ 1 if c == flip else z + 2 * (z % 2) - 1), y, c

    return lax.ppermute(block, "sp", sp_route(to))


def z_second(block):
    return z_first(block, 1)


def y_first(block, flip=0):
    return lax.ppermute(block, "sp", sp_route(lambda z, y, c: (z, y ^ (1 if c == flip else 3), c)))


def y_second(block):
    return y_first(block, 1)


def x_first(block, flip=0):
    count = lax.axis_size("tp")
    pairs = []
    for i in range(lax.axis_size("sp") * count):
        x, c = i % count, i // count % 2
        pairs.append((i, i - x + (x ^ (1 if c == flip else 3))))
    return lax.ppermute(block, ("sp", "tp"), pairs)


def x_second(block):
    return x_first(block, 1)


def swap(block):
    return lax.ppermute(block, "sp", sp_route(lambda z, y, c: (z, y, 1 - c)))


def from_behind(block, axis, distance):
    devices = range(lax.axis_size(axis))
    route = [(i - distance, i) for i in devices if i - distance in devices]
    return lax.ppermute(block, axis, route)


def z_at(z, core, i):
    sign = (1 - 2 * (z % 2)) * (1 - 2 * core)
    steps = (0, sign, 2 * sign, 3 * sign, -sign, -2 * sign, -3 * sign, 4)
    return (z + steps[i] + Z) % Z


def y_at(y, core, j):
    one = 1 + 2 * core
    return y ^ (0, one, one ^ 2, 2)[j]


def stack_body(place, *refs, n_in, along_z):
    out = refs[n_in]
    for i, ref in enumerate(refs[:n_in]):
        if along_z:
            at = z_at(place[0], place[2], i)
        else:
            at = y_at(place[1], place[2], i)
        out[at] = ref[:, : out.shape[2]]


def stack(place, pieces, along_z, width):
    rows = pieces[0].shape[0]
    return call(
        functools.partial(stack_body, n_in=len(pieces), along_z=along_z),
        jax.ShapeDtypeStruct((len(pieces), rows, width), pieces[0].dtype),
        (place, *pieces),
        [SMEM] + [VMEM] * len(pieces),
        4 * 10**8,
        6,
    )


def z_ring(block):
    first, second = [z_first(block)], [z_second(block)]
    for _ in range(2):
        f, s = z_first(second[-1]), z_second(first[-1])
        first.append(f)
        second.append(s)
    return [block, *first, *second, z_first(second[-1])]


def y_ring(block):
    first, second = y_first(block), y_second(block)
    return [block, first, second, y_first(second)]


def gathered_up(place, shard):
    own = z_ring(stack(place, y_ring(shard), False, NEAR))
    return own + [swap(p) for p in own]


def gathered_down(place, shard):
    own = y_ring(stack(place, z_ring(shard), True, shard.shape[1]))
    return own + [swap(p) for p in own]


def attend_body(info, sinks, q_in, k, v, halo, w_in, *rest, rows):
    outs, (k_ext, v_ext, q, w, sems, logits, weights, attended) = rest[:-8], rest[-8:]
    tokens = k.shape[0]
    copies = [
        pltpu.make_async_copy(src, dst, sems.at[i])
        for i, (src, dst) in enumerate(
            (
                (k, k_ext.at[WINDOW : WINDOW + tokens]),
                (q_in, q),
                (halo.at[0], k_ext.at[:WINDOW]),
                (v, v_ext.at[WINDOW : WINDOW + tokens]),
                (halo.at[1], v_ext.at[:WINDOW]),
                (w_in, w),
            )
        )
    ]
    for copy in copies:
        copy.start()
    rank, offset, core = info[0], info[1], info[2]
    one = 1 + 2 * core
    plan = [(rel, half) for rel in (2, one, one ^ 2, 0) for half in range(2)]
    for copy in copies[:3]:
        copy.wait()
    group = sinks.shape[0]
    span = rows + WINDOW

    def start_of(rel, half):
        return pl.multiple_of((rank ^ rel) * (2 * rows) + half * rows, rows)

    for at, (rel, half) in enumerate(plan):
        start = start_of(rel, half)
        key = k_ext[pl.ds(start, span), :]
        query = jnp.concatenate(
            [q[pl.ds(start, rows), g * HEAD : (g + 1) * HEAD] for g in range(group)], axis=0
        )
        logits[at] = lax.dot_general(
            query, key, (((1,), (1,)), ((), ())), preferred_element_type=jnp.float32
        )
    shape = (rows, span)
    q_index = lax.broadcasted_iota(jnp.int32, shape, 0)
    k_index = lax.broadcasted_iota(jnp.int32, shape, 1)
    dist = q_index + WINDOW - k_index
    in_window = (dist >= 0) & (dist < WINDOW)
    dist_f = dist.astype(jnp.float32)
    bias = []
    for g in range(group):
        head = jnp.full(shape, rank * group + g, jnp.int32).astype(jnp.float32)
        slope = jnp.exp2(-8.0 * (head + 1.0) / HEADS)
        bias.append(jnp.where(in_window, slope * dist_f, -neg_big))
    for at, (rel, half) in enumerate(plan):
        ahead = WINDOW - offset - start_of(rel, half)
        for g in range(group):
            part = logits[at, g * rows : (g + 1) * rows, :] * HEAD ** (-0.5) - bias[g]
            part = jnp.where(k_index < ahead, neg_big, part)
            top = jnp.maximum(jnp.max(part, axis=-1, keepdims=True), sinks[g])
            probs = jnp.exp(part - top)
            denom = jnp.sum(probs, axis=-1, keepdims=True) + jnp.exp(sinks[g] - top)
            weights[at, g * rows : (g + 1) * rows, :] = (probs * (1.0 / denom)).astype(
                jnp.bfloat16
            )
    for copy in copies[3:]:
        copy.wait()
    for at, (rel, half) in enumerate(plan):
        val = v_ext[pl.ds(start_of(rel, half), span), :]
        mixed = jnp.dot(weights[at], val, preferred_element_type=jnp.float32).astype(jnp.bfloat16)
        for g in range(group):
            attended[at * rows : (at + 1) * rows, g * HEAD : (g + 1) * HEAD] = mixed[
                g * rows : (g + 1) * rows
            ]
    step = 256

    def project(n, carry):
        cols = pl.ds(pl.multiple_of(n * step, step), step)
        mix = jnp.dot(attended[...], w[:, cols], preferred_element_type=jnp.float32).astype(
            jnp.bfloat16
        )
        at = 0
        for out in outs:
            out[:, cols] = mix[at : at + out.shape[0]]
            at += out.shape[0]
        return carry

    lax.fori_loop(0, w.shape[1] // step, project, 0)


def attend(info, sinks, q, k, v, halo, w, rows):
    width = w.shape[1]
    ext = pltpu.VMEM((k.shape[0] + WINDOW, HEAD), jnp.bfloat16)
    tall, span = sinks.shape[0] * rows, rows + WINDOW
    return call(
        functools.partial(attend_body, rows=rows),
        [jax.ShapeDtypeStruct((2 * rows, width), jnp.bfloat16)] * 4,
        (info, sinks, q, k, v, halo, w),
        [SMEM] * 2 + [HBM] * 5,
        6 * 10**9,
        54,
        [
            ext,
            ext,
            pltpu.VMEM(q.shape, jnp.bfloat16),
            pltpu.VMEM(w.shape, jnp.bfloat16),
            pltpu.SemaphoreType.DMA((6,)),
            pltpu.VMEM((8, tall, span), jnp.float32),
            pltpu.VMEM((8, tall, span), jnp.bfloat16),
            pltpu.VMEM((8 * rows, w.shape[0]), jnp.bfloat16),
        ],
    )


def norm(stream, gain, bias, *shares):
    mix = functools.reduce(lambda a, b: a + b, (p.astype(jnp.float32) for p in shares))
    value = deep_alpha * stream.astype(jnp.float32) + mix
    mean = jnp.mean(value, axis=-1, keepdims=True)
    spread = jnp.mean(jnp.square(value - mean), axis=-1, keepdims=True)
    return ((value - mean) * lax.rsqrt(spread + norm_eps) * gain + bias).astype(jnp.bfloat16)


def place_weights(place, ups, downs, up, down, sems):
    z, y, c = place[0], place[1], place[2]
    hidden, near = up.shape[-1], ups[0].shape[-1]

    def start_up():
        for side in range(2):
            core = c ^ side
            for j in range(Y):
                pltpu.make_async_copy(
                    downs[side * Y + j].at[:, :, hidden:],
                    up.at[:, y_at(y, core, j), core, :, near:],
                    sems.at[0],
                ).start()
            for i in range(Z):
                pltpu.make_async_copy(
                    ups[side * Z + i], up.at[z_at(z, core, i), :, core, :, :near], sems.at[0]
                ).start()

    def start_down():
        for side in range(2):
            core = c ^ side
            for j in range(Y):
                pltpu.make_async_copy(
                    downs[side * Y + j].at[:, :, :hidden],
                    down.at[:, y_at(y, core, j), core],
                    sems.at[1],
                ).start()

    return start_up, start_down


def ffn_rows(xs, outs, up, down, act, ready_up, ready_down):
    step = 256
    width = up.shape[-1]
    x = jnp.concatenate([r[...] for r in xs], axis=0) if len(xs) > 1 else xs[0][...]
    ready_up()

    def raise_(n, carry):
        cols = pl.ds(pl.multiple_of(n * step, step), step)
        w = up[:, :, :, :, cols].reshape(-1, step)
        upward = jnp.dot(x, w, preferred_element_type=jnp.float32)
        act[:, cols] = jnp.square(jnp.maximum(upward, 0.0)).astype(jnp.bfloat16)
        return carry

    lax.fori_loop(0, width // step, raise_, 0)
    ready_down()
    a = act[...]
    z_step = step // (down.shape[1] * down.shape[2] * down.shape[3])

    def lower(n, carry):
        w = down[pl.ds(n * z_step, z_step)].reshape(step, width)
        part = lax.dot_general(
            a, w, (((1,), (1,)), ((), ())), preferred_element_type=jnp.float32
        ).astype(jnp.bfloat16)
        cols = pl.ds(pl.multiple_of(n * step, step), step)
        at = 0
        for out in outs:
            out[:, cols] = part[at : at + out.shape[0]]
            at += out.shape[0]
        return carry

    lax.fori_loop(0, down.shape[0] // z_step, lower, 0)


def ffn_body(place, *refs, n_in, n_out, n_up, n_down):
    xs, refs = refs[:n_in], refs[n_in:]
    ups, downs, refs = refs[:n_up], refs[n_up : n_up + n_down], refs[n_up + n_down :]
    outs, (up, down, act, sems) = refs[:n_out], refs[n_out:]
    start_up, start_down = place_weights(place, ups, downs, up, down, sems)

    def ready_up():
        pltpu.make_async_copy(up, up, sems.at[0]).wait()
        start_down()

    def ready_down():
        pltpu.make_async_copy(down, down, sems.at[1]).wait()

    start_up()
    ffn_rows(xs, outs, up, down, act, ready_up, ready_down)


def ffn(place, xs, counts, ups, downs, hidden):
    rows = sum(x.shape[0] for x in xs)
    width = xs[0].shape[1]
    out, at = [], 0
    for n in counts:
        height = sum(x.shape[0] for x in xs[at : at + n])
        out.append(jax.ShapeDtypeStruct((height, width), jnp.bfloat16))
        at += n
    weights = pltpu.VMEM((Z, Y, 2, width // (Z * Y * 2), hidden), jnp.bfloat16)
    return call(
        functools.partial(ffn_body, n_in=len(xs), n_out=len(counts), n_up=len(ups), n_down=len(downs)),
        out,
        (place, *xs, *ups, *downs),
        [SMEM] + [VMEM] * len(xs) + [HBM] * (len(ups) + len(downs)),
        4 * rows * width * hidden,
        28,
        [weights, weights, pltpu.VMEM((rows, hidden), jnp.bfloat16), pltpu.SemaphoreType.DMA((2,))],
    )


def add(a, b):
    return (a.astype(jnp.float32) + b.astype(jnp.float32)).astype(jnp.bfloat16)


def on_device(
    queries, keys, values, residual, sinks, out_weight, up_weight, down_weight, gains, biases
):
    tokens = queries.shape[0]
    rows = residual.shape[0] // 2
    hidden = up_weight.shape[1]
    rank = lax.axis_index("tp")
    s = lax.axis_index("sp")
    place = jnp.stack([s // (2 * Y), s // 2 % Y, s % 2])

    tails = jnp.stack([keys[tokens - WINDOW :], values[tokens - WINDOW :]])
    halo = from_behind(tails, "sp", 1)
    ups = gathered_up(place, up_weight)
    downs = gathered_down(
        place, jnp.concatenate([down_weight.T, up_weight[:, NEAR:]], axis=1)
    )

    info = jnp.stack([rank, s * tokens, s % 2])
    far, first, second, own = attend(info, sinks, queries, keys, values, halo, out_weight, rows)
    from_far = x_first(far)
    from_first = x_first(first)
    from_second = x_second(add(second, from_far))
    normed = norm(residual, gains[0], biases[0], own, from_first, from_second)
    first = x_first(normed)
    second = [x_second(normed[:rows]), x_second(normed[rows:])]
    far = [x_first(second[0]), x_first(second[1])]
    far, first = ffn(place, (*far, first), (2, 1), ups, downs, hidden)
    from_far = x_first(far)
    from_first = x_first(first)
    second, own = ffn(place, (*second, normed), (2, 1), ups, downs, hidden)
    from_second = x_second(add(second, from_far))
    return norm(normed, gains[1], biases[1], own, from_first, from_second)


def solution(mesh):
    return jax.shard_map(
        on_device,
        mesh=mesh,
        in_specs=(
            P("sp", "tp"),
            P("sp", "tp"),
            P("sp", "tp"),
            P(("sp", "tp"), None),
            P("tp"),
            P("tp", None),
            P("sp", "tp"),
            P("tp", "sp"),
            P(),
            P(),
        ),
        out_specs=P(("sp", "tp"), None),
        check_vma=False,
    )
```

profile of v0, /device:TPU:1, one launch (start us, length us, event | category | flops | bytes accessed | tf_op | source)
XLA Modules:
  0.0 166.7 jit_solution(5195709097851182334)
XLA Ops:
  0.0 0.8 slice_bitcast_fusion
  0.8 4.6 %collective-permute-start = (bf16[2,128,128]{2,1,0:T(8,128)(2,1)S(1)}, bf16[2,128,128]{2,1,0:T(8,128)(2,1)S(1)}, u32[]{:S(2)}, u32[]{:S(2)}) collective-permute-start(bf16[2,128,128]{2,1,0:T(8,128)(2,1)S(1)} %pad_maximum_fusion.1), channel_id=1, source_target_pairs={{0,4},{4,8},{8,12},{12,16},{16,20},{20,24},{24,28},{28,32},{32,36}... | collective-permute-start | bytes 196616 | tf_op jit(solution)/shard_map/ppermute | solution.py:86
  5.4 0.7 add_add_fusion.2.info
  6.1 0.6 collective-permute-done.halo
  6.7 0.6 copy-done.6
  7.3 8.1 %shard_map.100 = (bf16[192,2048]{1,0:T(8,128)(2,1)}, bf16[192,2048]{1,0:T(8,128)(2,1)}, bf16[192,2048]{1,0:T(8,128)(2,1)}, bf16[192,2048]{1,0:T(8,128)(2,1)}) custom-call(s32[3]{0:T(128)} %add_add_fusion.2.info, f32[3]{0:T(128)} %sinks.1, bf16[768,384]{1,0:T(8,128)(2,1)} %q_in.1, bf16[768,128]{1,0:T(8,128)(2,1)} %k.1, bf16[768,128]{1,0:T(8,128)(2,1)} %v.1, ...), custom_call_target="tpu_custom_call" | custom-call | flops 6000000000 | tf_op jit(solution)/shard_map/pallas_call | solution.py:28
  15.5 2.6 %collective-permute-start.2 = (bf16[192,2048]{1,0:T(8,128)(2,1)}, bf16[192,2048]{1,0:T(8,128)(2,1)S(1)}, u32[]{:S(2)}, u32[]{:S(2)}) collective-permute-start(bf16[192,2048]{1,0:T(8,128)(2,1)} %get-tuple-element.16), channel_id=1, source_target_pairs={{0,1},{1,0},{2,3},{3,2},{4,7},{5,6},{6,5},{7,4},{8,9},{9,8},{10,11... | collective-permute-start | bytes 2359304 | tf_op jit(solution)/shard_map/ppermute | solution.py:72
  18.1 1.7 %collective-permute-start.25 = (bf16[32,2304]{1,0:T(8,128)(2,1)S(1)}, bf16[32,2304]{1,0:T(8,128)(2,1)S(1)}, u32[]{:S(2)}, u32[]{:S(2)}) collective-permute-start(bf16[32,2304]{1,0:T(8,128)(2,1)S(1)} %pad_maximum_fusion.refs_0_), channel_id=1, source_target_pairs={{0,224},{4,36},{8,232},{12,44},{16,240},{20,52},{24,248},{28,60},{... | collective-permute-start | bytes 442376 | tf_op jit(solution)/shard_map/ppermute | solution.py:51
  19.8 4.7 %collective-permute-start.24 = (bf16[32,2304]{1,0:T(8,128)(2,1)S(1)}, bf16[32,2304]{1,0:T(8,128)(2,1)S(1)}, u32[]{:S(2)}, u32[]{:S(2)}) collective-permute-start(bf16[32,2304]{1,0:T(8,128)(2,1)S(1)} %pad_maximum_fusion.refs_0_), channel_id=1, source_target_pairs={{0,32},{4,228},{8,40},{12,236},{16,48},{20,244},{24,56},{28,252},{... | collective-permute-start | bytes 442376 | tf_op jit(solution)/shard_map/ppermute | solution.py:51
  24.5 3.6 %collective-permute-start.26 = (bf16[32,2304]{1,0:T(8,128)(2,1)S(1)}, bf16[32,2304]{1,0:T(8,128)(2,1)S(1)}, u32[]{:S(2)}, u32[]{:S(2)}) collective-permute-start(bf16[32,2304]{1,0:T(8,128)(2,1)S(1)} %collective-permute-done.25.refs_4_), channel_id=1, source_target_pairs={{0,32},{4,228},{8,40},{12,236},{16,48},{20,244},{24,56},{28,252},{... | collective-permute-start | bytes 442376 | tf_op jit(solution)/shard_map/ppermute | solution.py:51
  28.0 2.1 %collective-permute-start.7 = (bf16[32,2048]{1,0:T(8,128)(2,1)S(1)}, bf16[32,2048]{1,0:T(8,128)(2,1)S(1)}, u32[]{:S(2)}, u32[]{:S(2)}) collective-permute-start(bf16[32,2048]{1,0:T(8,128)(2,1)S(1)} %copy-done), channel_id=1, source_target_pairs={{0,24},{4,12},{8,16},{12,4},{16,8},{20,28},{24,0},{28,20},{32,56},... | collective-permute-start | bytes 393224 | tf_op jit(solution)/shard_map/ppermute | solution.py:59
  30.1 1.3 collective-permute-start.6
  31.5 1.3 collective-permute-done.7.refs_2_
  32.8 1.0 collective-permute-start.8
  33.8 0.3 collective-permute-start.27
  34.2 1.1 collective-permute-start.29
  35.3 2.3 %add_convert_fusion.3 = bf16[192,2048]{1,0:T(8,128)(2,1)} fusion(bf16[192,2048]{1,0:T(8,128)(2,1)S(1)} %collective-permute-done.2, bf16[192,2048]{1,0:T(8,128)(2,1)} %get-tuple-element.15), kind=kLoop, calls=%fused_computation.7 | loop fusion | flops 1572864 | bytes 2359296 | tf_op jit(solution)/shard_map/convert_element_type | solution.py:365
  37.8 0.9 collective-permute-start.28
  38.8 0.6 collective-permute-done.29.refs_6_
  39.4 1.1 collective-permute-start.30
  40.6 0.6 shard_map.101.refs_3_
  41.3 3.3 %collective-permute-done.28.refs_3_ = bf16[32,2304]{1,0:T(8,128)(2,1)S(1)} collective-permute-done((bf16[32,2304]{1,0:T(8,128)(2,1)S(1)}, bf16[32,2304]{1,0:T(8,128)(2,1)S(1)}, u32[]{:S(2)}, u32[]{:S(2)}) %collective-permute-start.28) | collective-permute-done | bytes 147488 | tf_op jit(solution)/shard_map/ppermute | solution.py:51
  44.6 3.2 %collective-permute-done.30.refs_7_ = bf16[32,2304]{1,0:T(8,128)(2,1)S(1)} collective-permute-done((bf16[32,2304]{1,0:T(8,128)(2,1)S(1)}, bf16[32,2304]{1,0:T(8,128)(2,1)S(1)}, u32[]{:S(2)}, u32[]{:S(2)}) %collective-permute-start.30) | collective-permute-done | bytes 147488 | tf_op jit(solution)/shard_map/ppermute | solution.py:51
  47.7 0.6 shard_map.102.refs_19_
  48.3 1.7 %collective-permute-start.32 = (bf16[8,32,2304]{2,1,0:T(8,128)(2,1)S(1)}, bf16[8,32,2304]{2,1,0:T(8,128)(2,1)S(1)}, u32[]{:S(2)}, u32[]{:S(2)}) collective-permute-start(bf16[8,32,2304]{2,1,0:T(8,128)(2,1)S(1)} %shard_map.102.refs_19_), channel_id=1, source_target_pairs={{0,24},{4,12},{8,16},{12,4},{16,8},{20,28},{24,0},{28,20},{32,56},... | collective-permute-start | bytes 3538952 | tf_op jit(solution)/shard_map/ppermute | solution.py:59
  50.1 9.2 %collective-permute-start.16 = (bf16[4,32,1792]{2,1,0:T(8,128)(2,1)S(1)}, bf16[4,32,1792]{2,1,0:T(8,128)(2,1)S(1)}, u32[]{:S(2)}, u32[]{:S(2)}) collective-permute-start(bf16[4,32,1792]{2,1,0:T(8,128)(2,1)S(1)} %shard_map.101.refs_3_), channel_id=1, source_target_pairs={{0,4},{4,0},{8,12},{12,8},{16,20},{20,16},{24,28},{28,24},{32,36},... | collective-permute-start | bytes 1376264 | tf_op jit(solution)/shard_map/ppermute | solution.py:80
  59.3 1.8 %collective-permute-start.20 = (bf16[4,32,1792]{2,1,0:T(8,128)(2,1)S(1)}, bf16[4,32,1792]{2,1,0:T(8,128)(2,1)S(1)}, u32[]{:S(2)}, u32[]{:S(2)}) collective-permute-start(bf16[4,32,1792]{2,1,0:T(8,128)(2,1)S(1)} %collective-permute-done.10.refs_7_), channel_id=1, source_target_pairs={{0,4},{4,0},{8,12},{12,8},{16,20},{20,16},{24,28},{28,24},{32,36},... | collective-permute-start | bytes 1376264 | tf_op jit(solution)/shard_map/ppermute | solution.py:80
  61.1 1.2 collective-permute-start.11
  62.3 0.5 fusion
  62.9 0.6 collective-permute-start.12
  63.5 0.6 multiply_reduce_fusion.1
  64.1 1.8 %collective-permute-start.34 = (bf16[8,32,2304]{2,1,0:T(8,128)(2,1)S(1)}, bf16[8,32,2304]{2,1,0:T(8,128)(2,1)S(1)}, u32[]{:S(2)}, u32[]{:S(2)}) collective-permute-start(bf16[8,32,2304]{2,1,0:T(8,128)(2,1)S(1)} %shard_map.102.refs_19_), channel_id=1, source_target_pairs={{0,4},{4,0},{8,12},{12,8},{16,20},{20,16},{24,28},{28,24},{32,36},... | collective-permute-start | bytes 3538952 | tf_op jit(solution)/shard_map/ppermute | solution.py:80
  66.0 6.0 %collective-permute-done.11.refs_5_ = bf16[4,32,1792]{2,1,0:T(8,128)(2,1)S(1)} collective-permute-done((bf16[4,32,1792]{2,1,0:T(8,128)(2,1)S(1)}, bf16[4,32,1792]{2,1,0:T(8,128)(2,1)S(1)}, u32[]{:S(2)}, u32[]{:S(2)}) %collective-permute-start.11) | collective-permute-done | bytes 458784 | tf_op jit(solution)/shard_map/ppermute | solution.py:51
  72.1 3.5 %collective-permute-start.18 = (bf16[4,32,1792]{2,1,0:T(8,128)(2,1)S(1)}, bf16[4,32,1792]{2,1,0:T(8,128)(2,1)S(1)}, u32[]{:S(2)}, u32[]{:S(2)}) collective-permute-start(bf16[4,32,1792]{2,1,0:T(8,128)(2,1)S(1)} %collective-permute-done.11.refs_5_), channel_id=1, source_target_pairs={{0,4},{4,0},{8,12},{12,8},{16,20},{20,16},{24,28},{28,24},{32,36},... | collective-permute-start | bytes 1376264 | tf_op jit(solution)/shard_map/ppermute | solution.py:80
  75.7 0.8 add_convert_fusion.2.refs_2_
  76.4 0.6 collective-permute-done.18.refs_13_
  77.0 2.7 %collective-permute-start.21 = (bf16[4,32,1792]{2,1,0:T(8,128)(2,1)S(1)}, bf16[4,32,1792]{2,1,0:T(8,128)(2,1)S(1)}, u32[]{:S(2)}, u32[]{:S(2)}) collective-permute-start(bf16[4,32,1792]{2,1,0:T(8,128)(2,1)S(1)} %collective-permute-done.12.refs_8_), channel_id=1, source_target_pairs={{0,4},{4,0},{8,12},{12,8},{16,20},{20,16},{24,28},{28,24},{32,36},... | collective-permute-start | bytes 1376264 | tf_op jit(solution)/shard_map/ppermute | solution.py:80
  79.7 3.5 %collective-permute-done.14.refs_9_ = bf16[4,32,1792]{2,1,0:T(8,128)(2,1)S(1)} collective-permute-done((bf16[4,32,1792]{2,1,0:T(8,128)(2,1)S(1)}, bf16[4,32,1792]{2,1,0:T(8,128)(2,1)S(1)}, u32[]{:S(2)}, u32[]{:S(2)}) %collective-permute-start.14) | collective-permute-done | bytes 458784 | tf_op jit(solution)/shard_map/ppermute | solution.py:51
  83.2 1.2 collective-permute-start.13
  84.5 2.2 %collective-permute-start.5 = (bf16[96,2048]{1,0:T(8,128)(2,1)S(1)}, bf16[96,2048]{1,0:T(8,128)(2,1)S(1)}, u32[]{:S(2)}, u32[]{:S(2)}) collective-permute-start(bf16[96,2048]{1,0:T(8,128)(2,1)S(1)} %get-tuple-element.21), channel_id=1, source_target_pairs={{0,3},{1,2},{2,1},{3,0},{4,5},{5,4},{6,7},{7,6},{8,11},{9,10},{10,... | collective-permute-start | bytes 1179656 | tf_op jit(solution)/shard_map/ppermute | solution.py:72
  86.7 5.3 %collective-permute-done.13.refs_6_ = bf16[4,32,1792]{2,1,0:T(8,128)(2,1)S(1)} collective-permute-done((bf16[4,32,1792]{2,1,0:T(8,128)(2,1)S(1)}, bf16[4,32,1792]{2,1,0:T(8,128)(2,1)S(1)}, u32[]{:S(2)}, u32[]{:S(2)}) %collective-permute-start.13) | collective-permute-done | bytes 458784 | tf_op jit(solution)/shard_map/ppermute | solution.py:51
  92.0 1.8 %collective-permute-start.22 = (bf16[4,32,1792]{2,1,0:T(8,128)(2,1)S(1)}, bf16[4,32,1792]{2,1,0:T(8,128)(2,1)S(1)}, u32[]{:S(2)}, u32[]{:S(2)}) collective-permute-start(bf16[4,32,1792]{2,1,0:T(8,128)(2,1)S(1)} %collective-permute-done.14.refs_9_), channel_id=1, source_target_pairs={{0,4},{4,0},{8,12},{12,8},{16,20},{20,16},{24,28},{28,24},{32,36},... | collective-permute-start | bytes 1376264 | tf_op jit(solution)/shard_map/ppermute | solution.py:80
  93.9 1.2 collective-permute-start.15
  95.1 2.1 %collective-permute-start.4 = (bf16[96,2048]{1,0:T(8,128)(2,1)S(1)}, bf16[96,2048]{1,0:T(8,128)(2,1)S(1)}, u32[]{:S(2)}, u32[]{:S(2)}) collective-permute-start(bf16[96,2048]{1,0:T(8,128)(2,1)S(1)} %get-tuple-element.22), channel_id=1, source_target_pairs={{0,3},{1,2},{2,1},{3,0},{4,5},{5,4},{6,7},{7,6},{8,11},{9,10},{10,... | collective-permute-start | bytes 1179656 | tf_op jit(solution)/shard_map/ppermute | solution.py:72
  97.2 5.3 %collective-permute-done.4.refs_0_ = bf16[96,2048]{1,0:T(8,128)(2,1)S(1)} collective-permute-done((bf16[96,2048]{1,0:T(8,128)(2,1)S(1)}, bf16[96,2048]{1,0:T(8,128)(2,1)S(1)}, u32[]{:S(2)}, u32[]{:S(2)}) %collective-permute-start.4) | collective-permute-done | bytes 393248 | tf_op jit(solution)/shard_map/ppermute | solution.py:72
  102.6 1.0 collective-permute-start.39
  103.5 0.6 collective-permute-start.36
  104.2 0.3 collective-permute-start.35
  104.7 1.4 collective-permute-start.38
  106.1 4.3 %collective-permute-done.39.refs_1_ = bf16[96,2048]{1,0:T(8,128)(2,1)S(1)} collective-permute-done((bf16[96,2048]{1,0:T(8,128)(2,1)S(1)}, bf16[96,2048]{1,0:T(8,128)(2,1)S(1)}, u32[]{:S(2)}, u32[]{:S(2)}) %collective-permute-start.39) | collective-permute-done | bytes 393248 | tf_op jit(solution)/shard_map/ppermute | solution.py:72
  110.4 1.0 collective-permute-start.40
  111.4 3.3 %collective-permute-done.38.refs_0_ = bf16[96,2048]{1,0:T(8,128)(2,1)S(1)} collective-permute-done((bf16[96,2048]{1,0:T(8,128)(2,1)S(1)}, bf16[96,2048]{1,0:T(8,128)(2,1)S(1)}, u32[]{:S(2)}, u32[]{:S(2)}) %collective-permute-start.38) | collective-permute-done | bytes 393248 | tf_op jit(solution)/shard_map/ppermute | solution.py:72
  114.6 0.3 collective-permute-start.23
  114.9 8.1 %collective-permute-done.40.refs_2_ = bf16[192,2048]{1,0:T(8,128)(2,1)S(1)} collective-permute-done((bf16[192,2048]{1,0:T(8,128)(2,1)S(1)}, bf16[192,2048]{1,0:T(8,128)(2,1)S(1)}, u32[]{:S(2)}, u32[]{:S(2)}) %collective-permute-start.40) | collective-permute-done | bytes 786464 | tf_op jit(solution)/shard_map/ppermute | solution.py:72
  123.1 11.9 %shard_map.104 = (bf16[192,2048]{1,0:T(8,128)(2,1)S(1)}, bf16[192,2048]{1,0:T(8,128)(2,1)S(1)}) custom-call(s32[3]{0:T(128)S(1)} %add_add_fusion.3.place, bf16[96,2048]{1,0:T(8,128)(2,1)S(1)} %collective-permute-done.38.refs_0_, bf16[96,2048]{1,0:T(8,128)(2,1)S(1)} %collective-permute-done.39.refs_1_, bf16[192,2048]{1,0:T(8,128)(2,1)S(1)} %collective-permute-done.40.refs_2_, ...), custom_call_target="tpu_custom_call" | custom-call | flops 6442450944 | tf_op jit(solution)/shard_map/pallas_call | solution.py:28
  134.9 1.1 collective-permute-start.42
  136.0 1.7 %collective-permute-start.41 = (bf16[192,2048]{1,0:T(8,128)(2,1)S(1)}, bf16[192,2048]{1,0:T(8,128)(2,1)S(1)}, u32[]{:S(2)}, u32[]{:S(2)}) collective-permute-start(bf16[192,2048]{1,0:T(8,128)(2,1)S(1)} %get-tuple-element.18), channel_id=1, source_target_pairs={{0,1},{1,0},{2,3},{3,2},{4,7},{5,6},{6,5},{7,4},{8,9},{9,8},{10,11... | collective-permute-start | bytes 2359304 | tf_op jit(solution)/shard_map/ppermute | solution.py:72
  137.7 11.8 %shard_map.103 = (bf16[192,2048]{1,0:T(8,128)(2,1)S(1)}, bf16[192,2048]{1,0:T(8,128)(2,1)S(1)}) custom-call(s32[3]{0:T(128)S(1)} %add_add_fusion.3.place, bf16[96,2048]{1,0:T(8,128)(2,1)S(1)} %collective-permute-done.4.refs_0_, bf16[96,2048]{1,0:T(8,128)(2,1)S(1)} %collective-permute-done.5.refs_1_, bf16[192,2048]{1,0:T(8,128)(2,1)S(1)} %add_convert_fusion.2.refs_2_, ...), custom_call_target="tpu_custom_call" | custom-call | flops 6442450944 | tf_op jit(solution)/shard_map/pallas_call | solution.py:28
  149.6 0.3 add_convert_fusion.1
  149.9 7.7 %collective-permute-done.41 = bf16[192,2048]{1,0:T(8,128)(2,1)S(1)} collective-permute-done((bf16[192,2048]{1,0:T(8,128)(2,1)S(1)}, bf16[192,2048]{1,0:T(8,128)(2,1)S(1)}, u32[]{:S(2)}, u32[]{:S(2)}) %collective-permute-start.41) | collective-permute-done | bytes 786464 | tf_op jit(solution)/shard_map/ppermute | solution.py:72
  157.6 6.2 %collective-permute-done.43 = bf16[192,2048]{1,0:T(8,128)(2,1)S(1)} collective-permute-done((bf16[192,2048]{1,0:T(8,128)(2,1)S(1)}, bf16[192,2048]{1,0:T(8,128)(2,1)S(1)}, u32[]{:S(2)}, u32[]{:S(2)}) %collective-permute-start.43) | collective-permute-done | bytes 786464 | tf_op jit(solution)/shard_map/ppermute | solution.py:72
  163.8 0.5 fusion.1
  164.3 0.6 multiply_reduce_fusion
  165.0 1.7 add_convert_fusion
  (65 shorter events, 1.0 us)
Async XLA Ops:
  0.8 5.9 %collective-permute-start = (bf16[2,128,128]{2,1,0:T(8,128)(2,1)S(1)}, bf16[2,128,128]{2,1,0:T(8,128)(2,1)S(1)}, u32[]{:S(2)}, u32[]{:S(2)}) collective-permute-start(bf16[2,128,128]{2,1,0:T(8,128)(2,1)S(1)} %pad_maximum_fusion.1), channel_id=1, source_target_pairs={{0,4},{4,8},{8,12},{12,16},{16,20},{20,24},{24,28},{28,32},{32,36}... | collective-permute-start | bytes 196616 | tf_op jit(solution)/shard_map/ppermute | solution.py:86
  6.1 12.0 %slice-start = ((bf16[32,2048]{1,0:T(8,128)(2,1)}), bf16[32,256]{1,0:T(8,128)(2,1)S(1)}, s32[]{:S(2)}) async-start(bf16[32,2048]{1,0:T(8,128)(2,1)} %refs_0_.1), calls=%async_computation | async-start | bytes 32768 | tf_op jit(solution)/shard_map/slice | solution.py:382
  6.1 12.0 %copy-start.3 = (bf16[2048,32]{0,1:T(8,128)(2,1)S(1)}, bf16[2048,32]{0,1:T(8,128)(2,1)}, u32[]{:S(2)}) copy-start(bf16[2048,32]{0,1:T(8,128)(2,1)} %param.17) | copy-start | bytes 393220
  6.1 22.0 %copy-start = (bf16[32,2048]{1,0:T(8,128)(2,1)S(1)}, bf16[32,2048]{1,0:T(8,128)(2,1)}, u32[]{:S(2)}) copy-start(bf16[32,2048]{1,0:T(8,128)(2,1)} %refs_0_.1) | copy-start | bytes 393220
  6.7 0.6 copy-start.6
  15.5 22.1 %copy-start.4 = (f32[2,2048]{1,0:T(2,128)S(1)}, f32[2,2048]{1,0:T(2,128)}, u32[]{:S(2)}) copy-start(f32[2,2048]{1,0:T(2,128)} %param.18) | copy-start | bytes 49156
  15.5 18.7 %collective-permute-start.2 = (bf16[192,2048]{1,0:T(8,128)(2,1)}, bf16[192,2048]{1,0:T(8,128)(2,1)S(1)}, u32[]{:S(2)}, u32[]{:S(2)}) collective-permute-start(bf16[192,2048]{1,0:T(8,128)(2,1)} %get-tuple-element.16), channel_id=1, source_target_pairs={{0,1},{1,0},{2,3},{3,2},{4,7},{5,6},{6,5},{7,4},{8,9},{9,8},{10,11... | collective-permute-start | bytes 2359304 | tf_op jit(solution)/shard_map/ppermute | solution.py:72
  18.1 6.4 %collective-permute-start.25 = (bf16[32,2304]{1,0:T(8,128)(2,1)S(1)}, bf16[32,2304]{1,0:T(8,128)(2,1)S(1)}, u32[]{:S(2)}, u32[]{:S(2)}) collective-permute-start(bf16[32,2304]{1,0:T(8,128)(2,1)S(1)} %pad_maximum_fusion.refs_0_), channel_id=1, source_target_pairs={{0,224},{4,36},{8,232},{12,44},{16,240},{20,52},{24,248},{28,60},{... | collective-permute-start | bytes 442376 | tf_op jit(solution)/shard_map/ppermute | solution.py:51
  19.8 13.0 %collective-permute-start.24 = (bf16[32,2304]{1,0:T(8,128)(2,1)S(1)}, bf16[32,2304]{1,0:T(8,128)(2,1)S(1)}, u32[]{:S(2)}, u32[]{:S(2)}) collective-permute-start(bf16[32,2304]{1,0:T(8,128)(2,1)S(1)} %pad_maximum_fusion.refs_0_), channel_id=1, source_target_pairs={{0,32},{4,228},{8,40},{12,236},{16,48},{20,244},{24,56},{28,252},{... | collective-permute-start | bytes 442376 | tf_op jit(solution)/shard_map/ppermute | solution.py:51
  24.5 9.4 %collective-permute-start.26 = (bf16[32,2304]{1,0:T(8,128)(2,1)S(1)}, bf16[32,2304]{1,0:T(8,128)(2,1)S(1)}, u32[]{:S(2)}, u32[]{:S(2)}) collective-permute-start(bf16[32,2304]{1,0:T(8,128)(2,1)S(1)} %collective-permute-done.25.refs_4_), channel_id=1, source_target_pairs={{0,32},{4,228},{8,40},{12,236},{16,48},{20,244},{24,56},{28,252},{... | collective-permute-start | bytes 442376 | tf_op jit(solution)/shard_map/ppermute | solution.py:51
  28.0 4.8 %collective-permute-start.7 = (bf16[32,2048]{1,0:T(8,128)(2,1)S(1)}, bf16[32,2048]{1,0:T(8,128)(2,1)S(1)}, u32[]{:S(2)}, u32[]{:S(2)}) collective-permute-start(bf16[32,2048]{1,0:T(8,128)(2,1)S(1)} %copy-done), channel_id=1, source_target_pairs={{0,24},{4,12},{8,16},{12,4},{16,8},{20,28},{24,0},{28,20},{32,56},... | collective-permute-start | bytes 393224 | tf_op jit(solution)/shard_map/ppermute | solution.py:59
  30.1 7.4 %collective-permute-start.6 = (bf16[32,2048]{1,0:T(8,128)(2,1)S(1)}, bf16[32,2048]{1,0:T(8,128)(2,1)S(1)}, u32[]{:S(2)}, u32[]{:S(2)}) collective-permute-start(bf16[32,2048]{1,0:T(8,128)(2,1)S(1)} %copy-done), channel_id=1, source_target_pairs={{0,8},{4,28},{8,0},{12,20},{16,24},{20,12},{24,16},{28,4},{32,40},... | collective-permute-start | bytes 393224 | tf_op jit(solution)/shard_map/ppermute | solution.py:59
  32.8 28.3 %collective-permute-start.1 = (bf16[192,2048]{1,0:T(8,128)(2,1)}, bf16[192,2048]{1,0:T(8,128)(2,1)S(1)}, u32[]{:S(2)}, u32[]{:S(2)}) collective-permute-start(bf16[192,2048]{1,0:T(8,128)(2,1)} %get-tuple-element.14), channel_id=1, source_target_pairs={{0,1},{1,0},{2,3},{3,2},{4,7},{5,6},{6,5},{7,4},{8,9},{9,8},{10,11... | collective-permute-start | bytes 2359304 | tf_op jit(solution)/shard_map/ppermute | solution.py:72
  32.8 7.8 %collective-permute-start.8 = (bf16[32,2048]{1,0:T(8,128)(2,1)S(1)}, bf16[32,2048]{1,0:T(8,128)(2,1)S(1)}, u32[]{:S(2)}, u32[]{:S(2)}) collective-permute-start(bf16[32,2048]{1,0:T(8,128)(2,1)S(1)} %collective-permute-done.7.refs_2_), channel_id=1, source_target_pairs={{0,8},{4,28},{8,0},{12,20},{16,24},{20,12},{24,16},{28,4},{32,40},... | collective-permute-start | bytes 393224 | tf_op jit(solution)/shard_map/ppermute | solution.py:59
  33.8 4.0 %collective-permute-start.27 = (bf16[32,2304]{1,0:T(8,128)(2,1)S(1)}, bf16[32,2304]{1,0:T(8,128)(2,1)S(1)}, u32[]{:S(2)}, u32[]{:S(2)}) collective-permute-start(bf16[32,2304]{1,0:T(8,128)(2,1)S(1)} %collective-permute-done.24.refs_1_), channel_id=1, source_target_pairs={{0,224},{4,36},{8,232},{12,44},{16,240},{20,52},{24,248},{28,60},{... | collective-permute-start | bytes 442376 | tf_op jit(solution)/shard_map/ppermute | solution.py:51
  34.2 5.2 %collective-permute-start.29 = (bf16[32,2304]{1,0:T(8,128)(2,1)S(1)}, bf16[32,2304]{1,0:T(8,128)(2,1)S(1)}, u32[]{:S(2)}, u32[]{:S(2)}) collective-permute-start(bf16[32,2304]{1,0:T(8,128)(2,1)S(1)} %collective-permute-done.26.refs_2_), channel_id=1, source_target_pairs={{0,224},{4,36},{8,232},{12,44},{16,240},{20,52},{24,248},{28,60},{... | collective-permute-start | bytes 442376 | tf_op jit(solution)/shard_map/ppermute | solution.py:51
  37.6 24.7 %collective-permute-start.3 = (bf16[192,2048]{1,0:T(8,128)(2,1)}, bf16[192,2048]{1,0:T(8,128)(2,1)S(1)}, u32[]{:S(2)}, u32[]{:S(2)}) collective-permute-start(bf16[192,2048]{1,0:T(8,128)(2,1)} %add_convert_fusion.3), channel_id=1, source_target_pairs={{0,3},{1,2},{2,1},{3,0},{4,5},{5,4},{6,7},{7,6},{8,11},{9,10},{10,... | collective-permute-start | bytes 2359304 | tf_op jit(solution)/shard_map/ppermute | solution.py:72
  37.8 6.7 %collective-permute-start.28 = (bf16[32,2304]{1,0:T(8,128)(2,1)S(1)}, bf16[32,2304]{1,0:T(8,128)(2,1)S(1)}, u32[]{:S(2)}, u32[]{:S(2)}) collective-permute-start(bf16[32,2304]{1,0:T(8,128)(2,1)S(1)} %collective-permute-done.27.refs_5_), channel_id=1, source_target_pairs={{0,32},{4,228},{8,40},{12,236},{16,48},{20,244},{24,56},{28,252},{... | collective-permute-start | bytes 442376 | tf_op jit(solution)/shard_map/ppermute | solution.py:51
  39.4 8.3 %collective-permute-start.30 = (bf16[32,2304]{1,0:T(8,128)(2,1)S(1)}, bf16[32,2304]{1,0:T(8,128)(2,1)S(1)}, u32[]{:S(2)}, u32[]{:S(2)}) collective-permute-start(bf16[32,2304]{1,0:T(8,128)(2,1)S(1)} %collective-permute-done.29.refs_6_), channel_id=1, source_target_pairs={{0,32},{4,228},{8,40},{12,236},{16,48},{20,244},{24,56},{28,252},{... | collective-permute-start | bytes 442376 | tf_op jit(solution)/shard_map/ppermute | solution.py:51
  40.6 9.5 %copy-start.5 = (f32[2,2048]{1,0:T(2,128)S(1)}, f32[2,2048]{1,0:T(2,128)}, u32[]{:S(2)}) copy-start(f32[2,2048]{1,0:T(2,128)} %param.19) | copy-start | bytes 49156
  40.6 21.7 %copy-start.1 = (bf16[192,2048]{1,0:T(8,128)(2,1)S(1)}, bf16[192,2048]{1,0:T(8,128)(2,1)}, u32[]{:S(2)}) copy-start(bf16[192,2048]{1,0:T(8,128)(2,1)} %param.13) | copy-start | bytes 2359300
  40.6 21.7 %copy-start.2 = (bf16[192,2048]{1,0:T(8,128)(2,1)S(1)}, bf16[192,2048]{1,0:T(8,128)(2,1)}, u32[]{:S(2)}) copy-start(bf16[192,2048]{1,0:T(8,128)(2,1)} %get-tuple-element.13) | copy-start | bytes 2359300
  41.2 8.9 %collective-permute-start.10 = (bf16[4,32,1792]{2,1,0:T(8,128)(2,1)S(1)}, bf16[4,32,1792]{2,1,0:T(8,128)(2,1)S(1)}, u32[]{:S(2)}, u32[]{:S(2)}) collective-permute-start(bf16[4,32,1792]{2,1,0:T(8,128)(2,1)S(1)} %shard_map.101.refs_3_), channel_id=1, source_target_pairs={{0,224},{4,36},{8,232},{12,44},{16,240},{20,52},{24,248},{28,60},{... | collective-permute-start | bytes 1376264 | tf_op jit(solution)/shard_map/ppermute | solution.py:51
  44.5 14.8 %collective-permute-start.9 = (bf16[4,32,1792]{2,1,0:T(8,128)(2,1)S(1)}, bf16[4,32,1792]{2,1,0:T(8,128)(2,1)S(1)}, u32[]{:S(2)}, u32[]{:S(2)}) collective-permute-start(bf16[4,32,1792]{2,1,0:T(8,128)(2,1)S(1)} %shard_map.101.refs_3_), channel_id=1, source_target_pairs={{0,32},{4,228},{8,40},{12,236},{16,48},{20,244},{24,56},{28,252},{... | collective-permute-start | bytes 1376264 | tf_op jit(solution)/shard_map/ppermute | solution.py:51
  48.3 27.2 %collective-permute-start.32 = (bf16[8,32,2304]{2,1,0:T(8,128)(2,1)S(1)}, bf16[8,32,2304]{2,1,0:T(8,128)(2,1)S(1)}, u32[]{:S(2)}, u32[]{:S(2)}) collective-permute-start(bf16[8,32,2304]{2,1,0:T(8,128)(2,1)S(1)} %shard_map.102.refs_19_), channel_id=1, source_target_pairs={{0,24},{4,12},{8,16},{12,4},{16,8},{20,28},{24,0},{28,20},{32,56},... | collective-permute-start | bytes 3538952 | tf_op jit(solution)/shard_map/ppermute | solution.py:59
  50.1 12.8 %collective-permute-start.16 = (bf16[4,32,1792]{2,1,0:T(8,128)(2,1)S(1)}, bf16[4,32,1792]{2,1,0:T(8,128)(2,1)S(1)}, u32[]{:S(2)}, u32[]{:S(2)}) collective-permute-start(bf16[4,32,1792]{2,1,0:T(8,128)(2,1)S(1)} %shard_map.101.refs_3_), channel_id=1, source_target_pairs={{0,4},{4,0},{8,12},{12,8},{16,20},{20,16},{24,28},{28,24},{32,36},... | collective-permute-start | bytes 1376264 | tf_op jit(solution)/shard_map/ppermute | solution.py:80
  59.3 4.8 %collective-permute-start.20 = (bf16[4,32,1792]{2,1,0:T(8,128)(2,1)S(1)}, bf16[4,32,1792]{2,1,0:T(8,128)(2,1)S(1)}, u32[]{:S(2)}, u32[]{:S(2)}) collective-permute-start(bf16[4,32,1792]{2,1,0:T(8,128)(2,1)S(1)} %collective-permute-done.10.refs_7_), channel_id=1, source_target_pairs={{0,4},{4,0},{8,12},{12,8},{16,20},{20,16},{24,28},{28,24},{32,36},... | collective-permute-start | bytes 1376264 | tf_op jit(solution)/shard_map/ppermute | solution.py:80
  61.1 10.9 %collective-permute-start.11 = (bf16[4,32,1792]{2,1,0:T(8,128)(2,1)S(1)}, bf16[4,32,1792]{2,1,0:T(8,128)(2,1)S(1)}, u32[]{:S(2)}, u32[]{:S(2)}) collective-permute-start(bf16[4,32,1792]{2,1,0:T(8,128)(2,1)S(1)} %collective-permute-done.10.refs_7_), channel_id=1, source_target_pairs={{0,32},{4,228},{8,40},{12,236},{16,48},{20,244},{24,56},{28,252},{... | collective-permute-start | bytes 1376264 | tf_op jit(solution)/shard_map/ppermute | solution.py:51
  62.3 9.7 %collective-permute-start.17 = (bf16[4,32,1792]{2,1,0:T(8,128)(2,1)S(1)}, bf16[4,32,1792]{2,1,0:T(8,128)(2,1)S(1)}, u32[]{:S(2)}, u32[]{:S(2)}) collective-permute-start(bf16[4,32,1792]{2,1,0:T(8,128)(2,1)S(1)} %collective-permute-done.9.refs_4_), channel_id=1, source_target_pairs={{0,4},{4,0},{8,12},{12,8},{16,20},{20,16},{24,28},{28,24},{32,36},... | collective-permute-start | bytes 1376264 | tf_op jit(solution)/shard_map/ppermute | solution.py:80
  62.9 12.7 %collective-permute-start.12 = (bf16[4,32,1792]{2,1,0:T(8,128)(2,1)S(1)}, bf16[4,32,1792]{2,1,0:T(8,128)(2,1)S(1)}, u32[]{:S(2)}, u32[]{:S(2)}) collective-permute-start(bf16[4,32,1792]{2,1,0:T(8,128)(2,1)S(1)} %collective-permute-done.9.refs_4_), channel_id=1, source_target_pairs={{0,224},{4,36},{8,232},{12,44},{16,240},{20,52},{24,248},{28,60},{... | collective-permute-start | bytes 1376264 | tf_op jit(solution)/shard_map/ppermute | solution.py:51
  64.1 29.7 %collective-permute-start.34 = (bf16[8,32,2304]{2,1,0:T(8,128)(2,1)S(1)}, bf16[8,32,2304]{2,1,0:T(8,128)(2,1)S(1)}, u32[]{:S(2)}, u32[]{:S(2)}) collective-permute-start(bf16[8,32,2304]{2,1,0:T(8,128)(2,1)S(1)} %shard_map.102.refs_19_), channel_id=1, source_target_pairs={{0,4},{4,0},{8,12},{12,8},{16,20},{20,16},{24,28},{28,24},{32,36},... | collective-permute-start | bytes 3538952 | tf_op jit(solution)/shard_map/ppermute | solution.py:80
  72.0 23.0 %collective-permute-start.31 = (bf16[8,32,2304]{2,1,0:T(8,128)(2,1)S(1)}, bf16[8,32,2304]{2,1,0:T(8,128)(2,1)S(1)}, u32[]{:S(2)}, u32[]{:S(2)}) collective-permute-start(bf16[8,32,2304]{2,1,0:T(8,128)(2,1)S(1)} %shard_map.102.refs_19_), channel_id=1, source_target_pairs={{0,8},{4,28},{8,0},{12,20},{16,24},{20,12},{24,16},{28,4},{32,40},... | collective-permute-start | bytes 3538952 | tf_op jit(solution)/shard_map/ppermute | solution.py:59
  72.1 5.0 %collective-permute-start.18 = (bf16[4,32,1792]{2,1,0:T(8,128)(2,1)S(1)}, bf16[4,32,1792]{2,1,0:T(8,128)(2,1)S(1)}, u32[]{:S(2)}, u32[]{:S(2)}) collective-permute-start(bf16[4,32,1792]{2,1,0:T(8,128)(2,1)S(1)} %collective-permute-done.11.refs_5_), channel_id=1, source_target_pairs={{0,4},{4,0},{8,12},{12,8},{16,20},{20,16},{24,28},{28,24},{32,36},... | collective-permute-start | bytes 1376264 | tf_op jit(solution)/shard_map/ppermute | solution.py:80
  75.6 7.6 %collective-permute-start.14 = (bf16[4,32,1792]{2,1,0:T(8,128)(2,1)S(1)}, bf16[4,32,1792]{2,1,0:T(8,128)(2,1)S(1)}, u32[]{:S(2)}, u32[]{:S(2)}) collective-permute-start(bf16[4,32,1792]{2,1,0:T(8,128)(2,1)S(1)} %collective-permute-done.11.refs_5_), channel_id=1, source_target_pairs={{0,224},{4,36},{8,232},{12,44},{16,240},{20,52},{24,248},{28,60},{... | collective-permute-start | bytes 1376264 | tf_op jit(solution)/shard_map/ppermute | solution.py:51
  75.6 28.9 %collective-permute-start.33 = (bf16[8,32,2304]{2,1,0:T(8,128)(2,1)S(1)}, bf16[8,32,2304]{2,1,0:T(8,128)(2,1)S(1)}, u32[]{:S(2)}, u32[]{:S(2)}) collective-permute-start(bf16[8,32,2304]{2,1,0:T(8,128)(2,1)S(1)} %collective-permute-done.32.refs_21_), channel_id=1, source_target_pairs={{0,8},{4,28},{8,0},{12,20},{16,24},{20,12},{24,16},{28,4},{32,40},... | collective-permute-start | bytes 3538952 | tf_op jit(solution)/shard_map/ppermute | solution.py:59
  77.0 7.5 %collective-permute-start.21 = (bf16[4,32,1792]{2,1,0:T(8,128)(2,1)S(1)}, bf16[4,32,1792]{2,1,0:T(8,128)(2,1)S(1)}, u32[]{:S(2)}, u32[]{:S(2)}) collective-permute-start(bf16[4,32,1792]{2,1,0:T(8,128)(2,1)S(1)} %collective-permute-done.12.refs_8_), channel_id=1, source_target_pairs={{0,4},{4,0},{8,12},{12,8},{16,20},{20,16},{24,28},{28,24},{32,36},... | collective-permute-start | bytes 1376264 | tf_op jit(solution)/shard_map/ppermute | solution.py:80
  83.2 8.8 %collective-permute-start.13 = (bf16[4,32,1792]{2,1,0:T(8,128)(2,1)S(1)}, bf16[4,32,1792]{2,1,0:T(8,128)(2,1)S(1)}, u32[]{:S(2)}, u32[]{:S(2)}) collective-permute-start(bf16[4,32,1792]{2,1,0:T(8,128)(2,1)S(1)} %collective-permute-done.12.refs_8_), channel_id=1, source_target_pairs={{0,32},{4,228},{8,40},{12,236},{16,48},{20,244},{24,56},{28,252},{... | collective-permute-start | bytes 1376264 | tf_op jit(solution)/shard_map/ppermute | solution.py:51
  84.5 12.7 %collective-permute-start.5 = (bf16[96,2048]{1,0:T(8,128)(2,1)S(1)}, bf16[96,2048]{1,0:T(8,128)(2,1)S(1)}, u32[]{:S(2)}, u32[]{:S(2)}) collective-permute-start(bf16[96,2048]{1,0:T(8,128)(2,1)S(1)} %get-tuple-element.21), channel_id=1, source_target_pairs={{0,3},{1,2},{2,1},{3,0},{4,5},{5,4},{6,7},{7,6},{8,11},{9,10},{10,... | collective-permute-start | bytes 1179656 | tf_op jit(solution)/shard_map/ppermute | solution.py:72
  92.0 11.5 %collective-permute-start.22 = (bf16[4,32,1792]{2,1,0:T(8,128)(2,1)S(1)}, bf16[4,32,1792]{2,1,0:T(8,128)(2,1)S(1)}, u32[]{:S(2)}, u32[]{:S(2)}) collective-permute-start(bf16[4,32,1792]{2,1,0:T(8,128)(2,1)S(1)} %collective-permute-done.14.refs_9_), channel_id=1, source_target_pairs={{0,4},{4,0},{8,12},{12,8},{16,20},{20,16},{24,28},{28,24},{32,36},... | collective-permute-start | bytes 1376264 | tf_op jit(solution)/shard_map/ppermute | solution.py:80
  93.9 10.3 %collective-permute-start.15 = (bf16[4,32,1792]{2,1,0:T(8,128)(2,1)S(1)}, bf16[4,32,1792]{2,1,0:T(8,128)(2,1)S(1)}, u32[]{:S(2)}, u32[]{:S(2)}) collective-permute-start(bf16[4,32,1792]{2,1,0:T(8,128)(2,1)S(1)} %collective-permute-done.14.refs_9_), channel_id=1, source_target_pairs={{0,32},{4,228},{8,40},{12,236},{16,48},{20,244},{24,56},{28,252},{... | collective-permute-start | bytes 1376264 | tf_op jit(solution)/shard_map/ppermute | solution.py:51
  95.1 7.5 %collective-permute-start.4 = (bf16[96,2048]{1,0:T(8,128)(2,1)S(1)}, bf16[96,2048]{1,0:T(8,128)(2,1)S(1)}, u32[]{:S(2)}, u32[]{:S(2)}) collective-permute-start(bf16[96,2048]{1,0:T(8,128)(2,1)S(1)} %get-tuple-element.22), channel_id=1, source_target_pairs={{0,3},{1,2},{2,1},{3,0},{4,5},{5,4},{6,7},{7,6},{8,11},{9,10},{10,... | collective-permute-start | bytes 1179656 | tf_op jit(solution)/shard_map/ppermute | solution.py:72
  97.2 7.5 %collective-permute-start.19 = (bf16[4,32,1792]{2,1,0:T(8,128)(2,1)S(1)}, bf16[4,32,1792]{2,1,0:T(8,128)(2,1)S(1)}, u32[]{:S(2)}, u32[]{:S(2)}) collective-permute-start(bf16[4,32,1792]{2,1,0:T(8,128)(2,1)S(1)} %collective-permute-done.13.refs_6_), channel_id=1, source_target_pairs={{0,4},{4,0},{8,12},{12,8},{16,20},{20,16},{24,28},{28,24},{32,36},... | collective-permute-start | bytes 1376264 | tf_op jit(solution)/shard_map/ppermute | solution.py:80
  102.6 7.8 %collective-permute-start.39 = (bf16[96,2048]{1,0:T(8,128)(2,1)S(1)}, bf16[96,2048]{1,0:T(8,128)(2,1)S(1)}, u32[]{:S(2)}, u32[]{:S(2)}) collective-permute-start(bf16[96,2048]{1,0:T(8,128)(2,1)S(1)} %collective-permute-done.5.refs_1_), channel_id=1, source_target_pairs={{0,1},{1,0},{2,3},{3,2},{4,7},{5,6},{6,5},{7,4},{8,9},{9,8},{10,11... | collective-permute-start | bytes 1179656 | tf_op jit(solution)/shard_map/ppermute | solution.py:72
  103.5 19.5 %collective-permute-start.36 = (bf16[8,32,2304]{2,1,0:T(8,128)(2,1)S(1)}, bf16[8,32,2304]{2,1,0:T(8,128)(2,1)S(1)}, u32[]{:S(2)}, u32[]{:S(2)}) collective-permute-start(bf16[8,32,2304]{2,1,0:T(8,128)(2,1)S(1)} %collective-permute-done.32.refs_21_), channel_id=1, source_target_pairs={{0,4},{4,0},{8,12},{12,8},{16,20},{20,16},{24,28},{28,24},{32,36},... | collective-permute-start | bytes 3538952 | tf_op jit(solution)/shard_map/ppermute | solution.py:80
  104.2 18.9 %collective-permute-start.35 = (bf16[8,32,2304]{2,1,0:T(8,128)(2,1)S(1)}, bf16[8,32,2304]{2,1,0:T(8,128)(2,1)S(1)}, u32[]{:S(2)}, u32[]{:S(2)}) collective-permute-start(bf16[8,32,2304]{2,1,0:T(8,128)(2,1)S(1)} %collective-permute-done.31.refs_20_), channel_id=1, source_target_pairs={{0,4},{4,0},{8,12},{12,8},{16,20},{20,16},{24,28},{28,24},{32,36},... | collective-permute-start | bytes 3538952 | tf_op jit(solution)/shard_map/ppermute | solution.py:80
  104.5 18.6 %collective-permute-start.37 = (bf16[8,32,2304]{2,1,0:T(8,128)(2,1)S(1)}, bf16[8,32,2304]{2,1,0:T(8,128)(2,1)S(1)}, u32[]{:S(2)}, u32[]{:S(2)}) collective-permute-start(bf16[8,32,2304]{2,1,0:T(8,128)(2,1)S(1)} %collective-permute-done.33.refs_22_), channel_id=1, source_target_pairs={{0,4},{4,0},{8,12},{12,8},{16,20},{20,16},{24,28},{28,24},{32,36},... | collective-permute-start | bytes 3538952 | tf_op jit(solution)/shard_map/ppermute | solution.py:80
  104.7 9.9 %collective-permute-start.38 = (bf16[96,2048]{1,0:T(8,128)(2,1)S(1)}, bf16[96,2048]{1,0:T(8,128)(2,1)S(1)}, u32[]{:S(2)}, u32[]{:S(2)}) collective-permute-start(bf16[96,2048]{1,0:T(8,128)(2,1)S(1)} %collective-permute-done.4.refs_0_), channel_id=1, source_target_pairs={{0,1},{1,0},{2,3},{3,2},{4,7},{5,6},{6,5},{7,4},{8,9},{9,8},{10,11... | collective-permute-start | bytes 1179656 | tf_op jit(solution)/shard_map/ppermute | solution.py:72
  110.4 12.6 %collective-permute-start.40 = (bf16[192,2048]{1,0:T(8,128)(2,1)S(1)}, bf16[192,2048]{1,0:T(8,128)(2,1)S(1)}, u32[]{:S(2)}, u32[]{:S(2)}) collective-permute-start(bf16[192,2048]{1,0:T(8,128)(2,1)S(1)} %add_convert_fusion.2.refs_2_), channel_id=1, source_target_pairs={{0,1},{1,0},{2,3},{3,2},{4,7},{5,6},{6,5},{7,4},{8,9},{9,8},{10,11... | collective-permute-start | bytes 2359304 | tf_op jit(solution)/shard_map/ppermute | solution.py:72
  114.6 8.4 %collective-permute-start.23 = (bf16[4,32,1792]{2,1,0:T(8,128)(2,1)S(1)}, bf16[4,32,1792]{2,1,0:T(8,128)(2,1)S(1)}, u32[]{:S(2)}, u32[]{:S(2)}) collective-permute-start(bf16[4,32,1792]{2,1,0:T(8,128)(2,1)S(1)} %collective-permute-done.15.refs_10_), channel_id=1, source_target_pairs={{0,4},{4,0},{8,12},{12,8},{16,20},{20,16},{24,28},{28,24},{32,36},... | collective-permute-start | bytes 1376264 | tf_op jit(solution)/shard_map/ppermute | solution.py:80
  134.9 14.6 %collective-permute-start.42 = (bf16[192,2048]{1,0:T(8,128)(2,1)S(1)}, bf16[192,2048]{1,0:T(8,128)(2,1)S(1)}, u32[]{:S(2)}, u32[]{:S(2)}) collective-permute-start(bf16[192,2048]{1,0:T(8,128)(2,1)S(1)} %get-tuple-element.20), channel_id=1, source_target_pairs={{0,1},{1,0},{2,3},{3,2},{4,7},{5,6},{6,5},{7,4},{8,9},{9,8},{10,11... | collective-permute-start | bytes 2359304 | tf_op jit(solution)/shard_map/ppermute | solution.py:72
  136.0 21.6 %collective-permute-start.41 = (bf16[192,2048]{1,0:T(8,128)(2,1)S(1)}, bf16[192,2048]{1,0:T(8,128)(2,1)S(1)}, u32[]{:S(2)}, u32[]{:S(2)}) collective-permute-start(bf16[192,2048]{1,0:T(8,128)(2,1)S(1)} %get-tuple-element.18), channel_id=1, source_target_pairs={{0,1},{1,0},{2,3},{3,2},{4,7},{5,6},{6,5},{7,4},{8,9},{9,8},{10,11... | collective-permute-start | bytes 2359304 | tf_op jit(solution)/shard_map/ppermute | solution.py:72
  149.8 14.0 %collective-permute-start.43 = (bf16[192,2048]{1,0:T(8,128)(2,1)S(1)}, bf16[192,2048]{1,0:T(8,128)(2,1)S(1)}, u32[]{:S(2)}, u32[]{:S(2)}) collective-permute-start(bf16[192,2048]{1,0:T(8,128)(2,1)S(1)} %add_convert_fusion.1), channel_id=1, source_target_pairs={{0,3},{1,2},{2,1},{3,0},{4,5},{5,4},{6,7},{7,6},{8,11},{9,10},{10,... | collective-permute-start | bytes 2359304 | tf_op jit(solution)/shard_map/ppermute | solution.py:72
where the time goes:
time: 167 us
  starting transfers between devices  64.1 us (38%)
  waiting for transfers between devices  59.6 us (36%)
  Pallas kernels  33.1 us (20%)
  other arithmetic  8.1 us (5%)
    ppermute x11, waiting for transfers between devices, x_first(): return lax.ppermute(block, ('sp', 'tp'), pairs)  34.9 us
    pallas_call x5, Pallas kernels, call(): pl.pallas_call(body, out_shape=outs, in_specs=specs, out_specs=jax.tree.m...  33.1 us
    ppermute x12, starting transfers between devices, swap(): return lax.ppermute(block, 'sp', sp_route(lambda z, y, c: (z, y, 1 - c)))  22.3 us
    ppermute x14, waiting for transfers between devices, z_first(): return lax.ppermute(block, 'sp', sp_route(to))  22.1 us
    ppermute x14, starting transfers between devices, z_first(): return lax.ppermute(block, 'sp', sp_route(to))  17.8 us
    ppermute x11, starting transfers between devices, x_first(): return lax.ppermute(block, ('sp', 'tp'), pairs)  13.1 us
    ppermute x6, starting transfers between devices, y_first(): lax.ppermute(block, 'sp', sp_route(lambda z, y, c: (z, y ^ (1 if c == fli...  6.26 us
    ppermute x1, starting transfers between devices, from_behind(): return lax.ppermute(block, axis, route)  4.58 us
  transfers between devices with their start and end apart: 44, of which 16 were waited for; matrix products, arithmetic and copies ran while one was open for 3% of the time, Pallas kernels for 8%

commit v1 on v0

--- a/solution.py
+++ b/solution.py
@@ -12,7 +12,6 @@
 HEAD = 128
 WINDOW = 128
 Y, Z = 4, 8
-NEAR = 1792
 
 deep_alpha = 1.6817928
 norm_eps = 1e-05
@@ -104,11 +103,11 @@
             at = z_at(place[0], place[2], i)
         else:
             at = y_at(place[1], place[2], i)
-        out[at] = ref[:, : out.shape[2]]
-
-
-def stack(place, pieces, along_z, width):
-    rows = pieces[0].shape[0]
+        out[at] = ref[...]
+
+
+def stack(place, pieces, along_z):
+    rows, width = pieces[0].shape
     return call(
         functools.partial(stack_body, n_in=len(pieces), along_z=along_z),
         jax.ShapeDtypeStruct((len(pieces), rows, width), pieces[0].dtype),
@@ -134,12 +133,12 @@
 
 
 def gathered_up(place, shard):
-    own = z_ring(stack(place, y_ring(shard), False, NEAR))
+    own = z_ring(stack(place, y_ring(shard), False))
     return own + [swap(p) for p in own]
 
 
 def gathered_down(place, shard):
-    own = y_ring(stack(place, z_ring(shard), True, shard.shape[1]))
+    own = y_ring(stack(place, z_ring(shard), True))
     return own + [swap(p) for p in own]
 
 
@@ -212,7 +211,7 @@
             attended[at * rows : (at + 1) * rows, g * HEAD : (g + 1) * HEAD] = mixed[
                 g * rows : (g + 1) * rows
             ]
-    step = 256
+    step = 512
 
     def project(n, carry):
         cols = pl.ds(pl.multiple_of(n * step, step), step)
@@ -262,20 +261,13 @@
 
 def place_weights(place, ups, downs, up, down, sems):
     z, y, c = place[0], place[1], place[2]
-    hidden, near = up.shape[-1], ups[0].shape[-1]
 
     def start_up():
         for side in range(2):
             core = c ^ side
-            for j in range(Y):
-                pltpu.make_async_copy(
-                    downs[side * Y + j].at[:, :, hidden:],
-                    up.at[:, y_at(y, core, j), core, :, near:],
-                    sems.at[0],
-                ).start()
             for i in range(Z):
                 pltpu.make_async_copy(
-                    ups[side * Z + i], up.at[z_at(z, core, i), :, core, :, :near], sems.at[0]
+                    ups[side * Z + i], up.at[z_at(z, core, i), :, core], sems.at[0]
                 ).start()
 
     def start_down():
@@ -283,7 +275,7 @@
             core = c ^ side
             for j in range(Y):
                 pltpu.make_async_copy(
-                    downs[side * Y + j].at[:, :, :hidden],
+                    downs[side * Y + j],
                     down.at[:, y_at(y, core, j), core],
                     sems.at[1],
                 ).start()
@@ -292,7 +284,7 @@
 
 
 def ffn_rows(xs, outs, up, down, act, ready_up, ready_down):
-    step = 256
+    step = 512
     width = up.shape[-1]
     x = jnp.concatenate([r[...] for r in xs], axis=0) if len(xs) > 1 else xs[0][...]
     ready_up()
@@ -324,10 +316,10 @@
     lax.fori_loop(0, down.shape[0] // z_step, lower, 0)
 
 
-def ffn_body(place, *refs, n_in, n_out, n_up, n_down):
+def ffn_body(place, *refs, n_in, n_up, n_down):
     xs, refs = refs[:n_in], refs[n_in:]
     ups, downs, refs = refs[:n_up], refs[n_up : n_up + n_down], refs[n_up + n_down :]
-    outs, (up, down, act, sems) = refs[:n_out], refs[n_out:]
+    outs, (up, down, act, sems) = refs[:n_in], refs[n_in:]
     start_up, start_down = place_weights(place, ups, downs, up, down, sems)
 
     def ready_up():
@@ -341,17 +333,13 @@
     ffn_rows(xs, outs, up, down, act, ready_up, ready_down)
 
 
-def ffn(place, xs, counts, ups, downs, hidden):
+def ffn(place, xs, ups, downs, hidden):
     rows = sum(x.shape[0] for x in xs)
     width = xs[0].shape[1]
-    out, at = [], 0
-    for n in counts:
-        height = sum(x.shape[0] for x in xs[at : at + n])
-        out.append(jax.ShapeDtypeStruct((height, width), jnp.bfloat16))
-        at += n
+    out = [jax.ShapeDtypeStruct(x.shape, jnp.bfloat16) for x in xs]
     weights = pltpu.VMEM((Z, Y, 2, width // (Z * Y * 2), hidden), jnp.bfloat16)
     return call(
-        functools.partial(ffn_body, n_in=len(xs), n_out=len(counts), n_up=len(ups), n_down=len(downs)),
+        functools.partial(ffn_body, n_in=len(xs), n_up=len(ups), n_down=len(downs)),
         out,
         (place, *xs, *ups, *downs),
         [SMEM] + [VMEM] * len(xs) + [HBM] * (len(ups) + len(downs)),
@@ -378,9 +366,7 @@
     tails = jnp.stack([keys[tokens - WINDOW :], values[tokens - WINDOW :]])
     halo = from_behind(tails, "sp", 1)
     ups = gathered_up(place, up_weight)
-    downs = gathered_down(
-        place, jnp.concatenate([down_weight.T, up_weight[:, NEAR:]], axis=1)
-    )
+    downs = gathered_down(place, down_weight.T)
 
     info = jnp.stack([rank, s * tokens, s % 2])
     far, first, second, own = attend(info, sinks, queries, keys, values, halo, out_weight, rows)
@@ -389,12 +375,13 @@
     from_second = x_second(add(second, from_far))
     normed = norm(residual, gains[0], biases[0], own, from_first, from_second)
     first = x_first(normed)
-    second = [x_second(normed[:rows]), x_second(normed[rows:])]
-    far = [x_first(second[0]), x_first(second[1])]
-    far, first = ffn(place, (*far, first), (2, 1), ups, downs, hidden)
+    second = x_second(normed)
+    far = x_first(second)
+    weights = (ups, downs, hidden)
+    far, first = ffn(place, (far, first), *weights)
     from_far = x_first(far)
     from_first = x_first(first)
-    second, own = ffn(place, (*second, normed), (2, 1), ups, downs, hidden)
+    second, own = ffn(place, (second, normed), *weights)
     from_second = x_second(add(second, from_far))
     return norm(normed, gains[1], biases[1], own, from_first, from_second)
 

time: 167 us -> 173 us (1.036)
  waiting for transfers between devices: 59.6 us -> 71.1 us
  Pallas kernels: 33.1 us -> 28.8 us
  other arithmetic: 8.1 us -> 6.13 us
    ppermute x14, waiting for transfers between devices: 22.1 us -> 30.2 us  [z_first(): return lax.ppermute(block, 'sp', sp_route(to))]
    pallas_call x5, Pallas kernels: 33.1 us -> 28.8 us  [call(): pl.pallas_call(body, out_shape=outs, in_specs=specs, out_specs=jax.tree.m...]
    ppermute x6, starting transfers between devices: 6.26 us -> 8.59 us  [y_first(): lax.ppermute(block, 'sp', sp_route(lambda z, y, c: (z, y ^ (1 if c == fli...]
    convert_element_type x2, other arithmetic: 2.55 us -> 0.54 us  [add(): return (a.astype(jnp.float32) + b.astype(jnp.float32)).astype(jnp.bfloat16)]
    ppermute x11 -> x9, starting transfers between devices: 13.1 us -> 11.3 us  [x_first(): return lax.ppermute(block, ('sp', 'tp'), pairs)]
    ppermute x11 -> x9, waiting for transfers between devices: 34.9 us -> 35.8 us  [x_first(): return lax.ppermute(block, ('sp', 'tp'), pairs)]
  transfers between devices with their start and end apart: 44 -> 42, of which waited for: 16 -> 17; matrix products, arithmetic and copies ran while one was open for 3% -> 2% of each run, Pallas kernels for 8% -> 7%
where the time goes in v1:
time: 173 us; the launch traced here: 172 us
  waiting for transfers between devices  71.1 us (41%)
  starting transfers between devices  64.6 us (37%)
  Pallas kernels  28.8 us (17%)
  other arithmetic  6.13 us (4%)
    ppermute x9, waiting for transfers between devices, x_first(): return lax.ppermute(block, ('sp', 'tp'), pairs)  35.8 us
    ppermute x14, waiting for transfers between devices, z_first(): return lax.ppermute(block, 'sp', sp_route(to))  30.2 us
    pallas_call x5, Pallas kernels, call(): pl.pallas_call(body, out_shape=outs, in_specs=specs, out_specs=jax.tree.m...  28.8 us
    ppermute x12, starting transfers between devices, swap(): return lax.ppermute(block, 'sp', sp_route(lambda z, y, c: (z, y, 1 - c)))  23.2 us
    ppermute x14, starting transfers between devices, z_first(): return lax.ppermute(block, 'sp', sp_route(to))  16.9 us
    ppermute x9, starting transfers between devices, x_first(): return lax.ppermute(block, ('sp', 'tp'), pairs)  11.3 us
    ppermute x6, starting transfers between devices, y_first(): lax.ppermute(block, 'sp', sp_route(lambda z, y, c: (z, y ^ (1 if c == fli...  8.59 us
    ppermute x1, starting transfers between devices, from_behind(): return lax.ppermute(block, axis, route)  4.58 us
  transfers between devices with their start and end apart: 42, of which 17 were waited for; matrix products, arithmetic and copies ran while one was open for 2% of the time, Pallas kernels for 7%

profile of v1, /device:TPU:1, one launch (start us, length us, event | category | flops | bytes accessed | tf_op | source)
XLA Modules:
  0.0 172.3 jit_solution(8763178313241783103)
XLA Ops:
  0.0 0.8 slice_bitcast_fusion
  0.8 4.6 %collective-permute-start = (bf16[2,128,128]{2,1,0:T(8,128)(2,1)S(1)}, bf16[2,128,128]{2,1,0:T(8,128)(2,1)S(1)}, u32[]{:S(2)}, u32[]{:S(2)}) collective-permute-start(bf16[2,128,128]{2,1,0:T(8,128)(2,1)S(1)} %pad_maximum_fusion), channel_id=1, source_target_pairs={{0,4},{4,8},{8,12},{12,16},{16,20},{20,24},{24,28},{28,32},{32,36}... | collective-permute-start | bytes 196616 | tf_op jit(solution)/shard_map/ppermute | solution.py:85
  5.4 0.7 add_add_fusion.2.info
  6.1 0.6 collective-permute-done.halo
  6.7 0.6 copy-done.7
  7.3 7.5 %shard_map.100 = (bf16[192,2048]{1,0:T(8,128)(2,1)}, bf16[192,2048]{1,0:T(8,128)(2,1)}, bf16[192,2048]{1,0:T(8,128)(2,1)}, bf16[192,2048]{1,0:T(8,128)(2,1)}) custom-call(s32[3]{0:T(128)} %add_add_fusion.2.info, f32[3]{0:T(128)} %sinks.1, bf16[768,384]{1,0:T(8,128)(2,1)} %q_in.1, bf16[768,128]{1,0:T(8,128)(2,1)} %k.1, bf16[768,128]{1,0:T(8,128)(2,1)} %v.1, ...), custom_call_target="tpu_custom_call" | custom-call | flops 6000000000 | tf_op jit(solution)/shard_map/pallas_call | solution.py:27
  14.8 2.6 %collective-permute-start.2 = (bf16[192,2048]{1,0:T(8,128)(2,1)}, bf16[192,2048]{1,0:T(8,128)(2,1)S(1)}, u32[]{:S(2)}, u32[]{:S(2)}) collective-permute-start(bf16[192,2048]{1,0:T(8,128)(2,1)} %get-tuple-element.16), channel_id=1, source_target_pairs={{0,1},{1,0},{2,3},{3,2},{4,7},{5,6},{6,5},{7,4},{8,9},{9,8},{10,11... | collective-permute-start | bytes 2359304 | tf_op jit(solution)/shard_map/ppermute | solution.py:71
  17.4 1.3 collective-permute-start.6
  18.7 1.6 collective-permute-start.24
  20.3 4.7 %collective-permute-start.23 = (bf16[32,2048]{1,0:T(8,128)(2,1)S(1)}, bf16[32,2048]{1,0:T(8,128)(2,1)S(1)}, u32[]{:S(2)}, u32[]{:S(2)}) collective-permute-start(bf16[32,2048]{1,0:T(8,128)(2,1)S(1)} %bitcast.15), channel_id=1, source_target_pairs={{0,32},{4,228},{8,40},{12,236},{16,48},{20,244},{24,56},{28,252},{... | collective-permute-start | bytes 393224 | tf_op jit(solution)/shard_map/ppermute | solution.py:50
  25.0 1.6 collective-permute-start.5
  26.6 1.1 collective-permute-start.7
  27.7 0.8 collective-permute-start.25
  28.7 1.4 collective-permute-done.5.refs_1_
  30.0 1.6 collective-permute-done.7.refs_3_
  31.7 0.6 shard_map.101.refs_2_
  32.2 0.1 collective-permute-start.9
  32.3 0.4 collective-permute-done.25.refs_2_
  32.7 1.1 collective-permute-start.28
  33.8 0.3 add_convert_fusion.3
  34.2 1.2 collective-permute-done.26.refs_5_
  35.4 0.4 collective-permute-start.27
  35.8 6.6 %collective-permute-done.28.refs_6_ = bf16[32,2048]{1,0:T(8,128)(2,1)S(1)} collective-permute-done((bf16[32,2048]{1,0:T(8,128)(2,1)S(1)}, bf16[32,2048]{1,0:T(8,128)(2,1)S(1)}, u32[]{:S(2)}, u32[]{:S(2)}) %collective-permute-start.28) | collective-permute-done | bytes 131104 | tf_op jit(solution)/shard_map/ppermute | solution.py:50
  42.5 2.0 %collective-permute-start.29 = (bf16[32,2048]{1,0:T(8,128)(2,1)S(1)}, bf16[32,2048]{1,0:T(8,128)(2,1)S(1)}, u32[]{:S(2)}, u32[]{:S(2)}) collective-permute-start(bf16[32,2048]{1,0:T(8,128)(2,1)S(1)} %collective-permute-done.28.refs_6_), channel_id=1, source_target_pairs={{0,32},{4,228},{8,40},{12,236},{16,48},{20,244},{24,56},{28,252},{... | collective-permute-start | bytes 393224 | tf_op jit(solution)/shard_map/ppermute | solution.py:50
  44.5 5.1 %collective-permute-start.15 = (bf16[4,32,2048]{2,1,0:T(8,128)(2,1)S(1)}, bf16[4,32,2048]{2,1,0:T(8,128)(2,1)S(1)}, u32[]{:S(2)}, u32[]{:S(2)}) collective-permute-start(bf16[4,32,2048]{2,1,0:T(8,128)(2,1)S(1)} %shard_map.101.refs_2_), channel_id=1, source_target_pairs={{0,4},{4,0},{8,12},{12,8},{16,20},{20,16},{24,28},{28,24},{32,36},... | collective-permute-start | bytes 1572872 | tf_op jit(solution)/shard_map/ppermute | solution.py:79
  49.6 2.1 %collective-permute-start.8 = (bf16[4,32,2048]{2,1,0:T(8,128)(2,1)S(1)}, bf16[4,32,2048]{2,1,0:T(8,128)(2,1)S(1)}, u32[]{:S(2)}, u32[]{:S(2)}) collective-permute-start(bf16[4,32,2048]{2,1,0:T(8,128)(2,1)S(1)} %shard_map.101.refs_2_), channel_id=1, source_target_pairs={{0,32},{4,228},{8,40},{12,236},{16,48},{20,244},{24,56},{28,252},{... | collective-permute-start | bytes 1572872 | tf_op jit(solution)/shard_map/ppermute | solution.py:50
  51.7 2.8 %collective-permute-start.19 = (bf16[4,32,2048]{2,1,0:T(8,128)(2,1)S(1)}, bf16[4,32,2048]{2,1,0:T(8,128)(2,1)S(1)}, u32[]{:S(2)}, u32[]{:S(2)}) collective-permute-start(bf16[4,32,2048]{2,1,0:T(8,128)(2,1)S(1)} %collective-permute-done.9.refs_6_), channel_id=1, source_target_pairs={{0,4},{4,0},{8,12},{12,8},{16,20},{20,16},{24,28},{28,24},{32,36},... | collective-permute-start | bytes 1572872 | tf_op jit(solution)/shard_map/ppermute | solution.py:79
  54.6 0.6 shard_map.102.refs_18_
  55.2 0.3 collective-permute-start.33
  55.5 3.3 %collective-permute-done.8.refs_3_ = bf16[4,32,2048]{2,1,0:T(8,128)(2,1)S(1)} collective-permute-done((bf16[4,32,2048]{2,1,0:T(8,128)(2,1)S(1)}, bf16[4,32,2048]{2,1,0:T(8,128)(2,1)S(1)}, u32[]{:S(2)}, u32[]{:S(2)}) %collective-permute-start.8) | collective-permute-done | bytes 524320 | tf_op jit(solution)/shard_map/ppermute | solution.py:50
  58.8 0.9 collective-permute-start.31
  59.7 0.3 collective-permute-start.30
  60.0 2.4 %collective-permute-start.10 = (bf16[4,32,2048]{2,1,0:T(8,128)(2,1)S(1)}, bf16[4,32,2048]{2,1,0:T(8,128)(2,1)S(1)}, u32[]{:S(2)}, u32[]{:S(2)}) collective-permute-start(bf16[4,32,2048]{2,1,0:T(8,128)(2,1)S(1)} %collective-permute-done.9.refs_6_), channel_id=1, source_target_pairs={{0,32},{4,228},{8,40},{12,236},{16,48},{20,244},{24,56},{28,252},{... | collective-permute-start | bytes 1572872 | tf_op jit(solution)/shard_map/ppermute | solution.py:50
  62.4 3.0 %collective-permute-start.16 = (bf16[4,32,2048]{2,1,0:T(8,128)(2,1)S(1)}, bf16[4,32,2048]{2,1,0:T(8,128)(2,1)S(1)}, u32[]{:S(2)}, u32[]{:S(2)}) collective-permute-start(bf16[4,32,2048]{2,1,0:T(8,128)(2,1)S(1)} %collective-permute-done.8.refs_3_), channel_id=1, source_target_pairs={{0,4},{4,0},{8,12},{12,8},{16,20},{20,16},{24,28},{28,24},{32,36},... | collective-permute-start | bytes 1572872 | tf_op jit(solution)/shard_map/ppermute | solution.py:79
  65.4 0.5 fusion
  66.0 3.6 %collective-permute-done.10.refs_4_ = bf16[4,32,2048]{2,1,0:T(8,128)(2,1)S(1)} collective-permute-done((bf16[4,32,2048]{2,1,0:T(8,128)(2,1)S(1)}, bf16[4,32,2048]{2,1,0:T(8,128)(2,1)S(1)}, u32[]{:S(2)}, u32[]{:S(2)}) %collective-permute-start.10) | collective-permute-done | bytes 524320 | tf_op jit(solution)/shard_map/ppermute | solution.py:50
  69.6 1.5 collective-permute-start.13
  71.0 0.7 multiply_reduce_fusion.1
  71.7 8.0 %collective-permute-done.11.refs_7_ = bf16[4,32,2048]{2,1,0:T(8,128)(2,1)S(1)} collective-permute-done((bf16[4,32,2048]{2,1,0:T(8,128)(2,1)S(1)}, bf16[4,32,2048]{2,1,0:T(8,128)(2,1)S(1)}, u32[]{:S(2)}, u32[]{:S(2)}) %collective-permute-start.11) | collective-permute-done | bytes 524320 | tf_op jit(solution)/shard_map/ppermute | solution.py:50
  79.7 7.0 %collective-permute-start.17 = (bf16[4,32,2048]{2,1,0:T(8,128)(2,1)S(1)}, bf16[4,32,2048]{2,1,0:T(8,128)(2,1)S(1)}, u32[]{:S(2)}, u32[]{:S(2)}) collective-permute-start(bf16[4,32,2048]{2,1,0:T(8,128)(2,1)S(1)} %collective-permute-done.10.refs_4_), channel_id=1, source_target_pairs={{0,4},{4,0},{8,12},{12,8},{16,20},{20,16},{24,28},{28,24},{32,36},... | collective-permute-start | bytes 1572872 | tf_op jit(solution)/shard_map/ppermute | solution.py:79
  86.8 3.4 %collective-permute-start.32 = (bf16[8,32,2048]{2,1,0:T(8,128)(2,1)S(1)}, bf16[8,32,2048]{2,1,0:T(8,128)(2,1)S(1)}, u32[]{:S(2)}, u32[]{:S(2)}) collective-permute-start(bf16[8,32,2048]{2,1,0:T(8,128)(2,1)S(1)} %collective-permute-done.31.refs_20_), channel_id=1, source_target_pairs={{0,8},{4,28},{8,0},{12,20},{16,24},{20,12},{24,16},{28,4},{32,40},... | collective-permute-start | bytes 3145736 | tf_op jit(solution)/shard_map/ppermute | solution.py:58
  90.2 3.2 %collective-permute-start.21 = (bf16[4,32,2048]{2,1,0:T(8,128)(2,1)S(1)}, bf16[4,32,2048]{2,1,0:T(8,128)(2,1)S(1)}, u32[]{:S(2)}, u32[]{:S(2)}) collective-permute-start(bf16[4,32,2048]{2,1,0:T(8,128)(2,1)S(1)} %collective-permute-done.13.refs_8_), channel_id=1, source_target_pairs={{0,4},{4,0},{8,12},{12,8},{16,20},{20,16},{24,28},{28,24},{32,36},... | collective-permute-start | bytes 1572872 | tf_op jit(solution)/shard_map/ppermute | solution.py:79
  93.5 0.8 add_convert_fusion.2.refs_1_
  94.4 2.8 %collective-permute-done.12.refs_5_ = bf16[4,32,2048]{2,1,0:T(8,128)(2,1)S(1)} collective-permute-done((bf16[4,32,2048]{2,1,0:T(8,128)(2,1)S(1)}, bf16[4,32,2048]{2,1,0:T(8,128)(2,1)S(1)}, u32[]{:S(2)}, u32[]{:S(2)}) %collective-permute-start.12) | collective-permute-done | bytes 524320 | tf_op jit(solution)/shard_map/ppermute | solution.py:50
  97.2 0.6 collective-permute-start.4
  97.8 2.0 %collective-permute-start.38 = (bf16[192,2048]{1,0:T(8,128)(2,1)S(1)}, bf16[192,2048]{1,0:T(8,128)(2,1)S(1)}, u32[]{:S(2)}, u32[]{:S(2)}) collective-permute-start(bf16[192,2048]{1,0:T(8,128)(2,1)S(1)} %add_convert_fusion.2.refs_1_), channel_id=1, source_target_pairs={{0,1},{1,0},{2,3},{3,2},{4,7},{5,6},{6,5},{7,4},{8,9},{9,8},{10,11... | collective-permute-start | bytes 2359304 | tf_op jit(solution)/shard_map/ppermute | solution.py:71
  99.7 4.2 %collective-permute-done.14.refs_9_ = bf16[4,32,2048]{2,1,0:T(8,128)(2,1)S(1)} collective-permute-done((bf16[4,32,2048]{2,1,0:T(8,128)(2,1)S(1)}, bf16[4,32,2048]{2,1,0:T(8,128)(2,1)S(1)}, u32[]{:S(2)}, u32[]{:S(2)}) %collective-permute-start.14) | collective-permute-done | bytes 524320 | tf_op jit(solution)/shard_map/ppermute | solution.py:50
  103.9 0.5 collective-permute-start.34
  104.5 9.1 %collective-permute-done.4.refs_0_ = bf16[192,2048]{1,0:T(8,128)(2,1)S(1)} collective-permute-done((bf16[192,2048]{1,0:T(8,128)(2,1)S(1)}, bf16[192,2048]{1,0:T(8,128)(2,1)S(1)}, u32[]{:S(2)}, u32[]{:S(2)}) %collective-permute-start.4) | collective-permute-done | bytes 786464 | tf_op jit(solution)/shard_map/ppermute | solution.py:71
  113.6 3.2 %collective-permute-start.37 = (bf16[192,2048]{1,0:T(8,128)(2,1)S(1)}, bf16[192,2048]{1,0:T(8,128)(2,1)S(1)}, u32[]{:S(2)}, u32[]{:S(2)}) collective-permute-start(bf16[192,2048]{1,0:T(8,128)(2,1)S(1)} %collective-permute-done.4.refs_0_), channel_id=1, source_target_pairs={{0,1},{1,0},{2,3},{3,2},{4,7},{5,6},{6,5},{7,4},{8,9},{9,8},{10,11... | collective-permute-start | bytes 2359304 | tf_op jit(solution)/shard_map/ppermute | solution.py:71
  116.8 1.4 collective-permute-done.38.refs_1_
  118.1 1.2 collective-permute-start.22
  119.4 1.5 collective-permute-done.22.refs_17_
  120.9 5.8 %collective-permute-done.37.refs_0_ = bf16[192,2048]{1,0:T(8,128)(2,1)S(1)} collective-permute-done((bf16[192,2048]{1,0:T(8,128)(2,1)S(1)}, bf16[192,2048]{1,0:T(8,128)(2,1)S(1)}, u32[]{:S(2)}, u32[]{:S(2)}) %collective-permute-start.37) | collective-permute-done | bytes 786464 | tf_op jit(solution)/shard_map/ppermute | solution.py:71
  126.7 10.0 %shard_map.104 = (bf16[192,2048]{1,0:T(8,128)(2,1)S(1)}, bf16[192,2048]{1,0:T(8,128)(2,1)S(1)}) custom-call(s32[3]{0:T(128)S(1)} %add_add_fusion.3.place, bf16[192,2048]{1,0:T(8,128)(2,1)S(1)} %collective-permute-done.37.refs_0_, bf16[192,2048]{1,0:T(8,128)(2,1)S(1)} %collective-permute-done.38.refs_1_, bf16[4,32,2048]{2,1,0:T(8,128)(2,1)S(1)} %shard_map.101.refs_2_, ...), custom_call_target="tpu_custom_call" | custom-call | flops 6442450944 | tf_op jit(solution)/shard_map/pallas_call | solution.py:27
  136.7 2.2 %collective-permute-start.40 = (bf16[192,2048]{1,0:T(8,128)(2,1)S(1)}, bf16[192,2048]{1,0:T(8,128)(2,1)S(1)}, u32[]{:S(2)}, u32[]{:S(2)}) collective-permute-start(bf16[192,2048]{1,0:T(8,128)(2,1)S(1)} %get-tuple-element.20), channel_id=1, source_target_pairs={{0,1},{1,0},{2,3},{3,2},{4,7},{5,6},{6,5},{7,4},{8,9},{9,8},{10,11... | collective-permute-start | bytes 2359304 | tf_op jit(solution)/shard_map/ppermute | solution.py:71
  139.0 0.5 collective-permute-start.39
  139.5 10.0 %shard_map.103 = (bf16[192,2048]{1,0:T(8,128)(2,1)S(1)}, bf16[192,2048]{1,0:T(8,128)(2,1)S(1)}) custom-call(s32[3]{0:T(128)S(1)} %add_add_fusion.3.place, bf16[192,2048]{1,0:T(8,128)(2,1)S(1)} %collective-permute-done.4.refs_0_, bf16[192,2048]{1,0:T(8,128)(2,1)S(1)} %add_convert_fusion.2.refs_1_, bf16[4,32,2048]{2,1,0:T(8,128)(2,1)S(1)} %shard_map.101.refs_2_, ...), custom_call_target="tpu_custom_call" | custom-call | flops 6442450944 | tf_op jit(solution)/shard_map/pallas_call | solution.py:27
  149.5 0.3 add_convert_fusion.1
  149.9 7.4 %collective-permute-done.39 = bf16[192,2048]{1,0:T(8,128)(2,1)S(1)} collective-permute-done((bf16[192,2048]{1,0:T(8,128)(2,1)S(1)}, bf16[192,2048]{1,0:T(8,128)(2,1)S(1)}, u32[]{:S(2)}, u32[]{:S(2)}) %collective-permute-start.39) | collective-permute-done | bytes 786464 | tf_op jit(solution)/shard_map/ppermute | solution.py:71
  157.3 12.2 %collective-permute-done.41 = bf16[192,2048]{1,0:T(8,128)(2,1)S(1)} collective-permute-done((bf16[192,2048]{1,0:T(8,128)(2,1)S(1)}, bf16[192,2048]{1,0:T(8,128)(2,1)S(1)}, u32[]{:S(2)}, u32[]{:S(2)}) %collective-permute-start.41) | collective-permute-done | bytes 786464 | tf_op jit(solution)/shard_map/ppermute | solution.py:71
  169.5 0.5 fusion.1
  170.0 0.6 multiply_reduce_fusion
  170.7 1.7 add_convert_fusion
  (59 shorter events, 0.8 us)
Async XLA Ops:
  0.8 5.9 %collective-permute-start = (bf16[2,128,128]{2,1,0:T(8,128)(2,1)S(1)}, bf16[2,128,128]{2,1,0:T(8,128)(2,1)S(1)}, u32[]{:S(2)}, u32[]{:S(2)}) collective-permute-start(bf16[2,128,128]{2,1,0:T(8,128)(2,1)S(1)} %pad_maximum_fusion), channel_id=1, source_target_pairs={{0,4},{4,8},{8,12},{12,16},{16,20},{20,24},{24,28},{28,32},{32,36}... | collective-permute-start | bytes 196616 | tf_op jit(solution)/shard_map/ppermute | solution.py:85
  6.1 11.3 %copy-start.1 = (bf16[32,2048]{1,0:T(8,128)(2,1)S(1)}, bf16[32,2048]{1,0:T(8,128)(2,1)}, u32[]{:S(2)}) copy-start(bf16[32,2048]{1,0:T(8,128)(2,1)} %refs_0_.1) | copy-start | bytes 393220
  6.1 12.6 %copy-start = (bf16[2048,32]{0,1:T(8,128)(2,1)S(1)}, bf16[2048,32]{0,1:T(8,128)(2,1)}, u32[]{:S(2)}) copy-start(bf16[2048,32]{0,1:T(8,128)(2,1)} %param.17) | copy-start | bytes 393220
  6.7 0.6 copy-start.7
  14.8 19.0 %copy-start.4 = (bf16[192,2048]{1,0:T(8,128)(2,1)S(1)}, bf16[192,2048]{1,0:T(8,128)(2,1)}, u32[]{:S(2)}) copy-start(bf16[192,2048]{1,0:T(8,128)(2,1)} %get-tuple-element.15) | copy-start | bytes 2359300
  14.8 19.0 %collective-permute-start.2 = (bf16[192,2048]{1,0:T(8,128)(2,1)}, bf16[192,2048]{1,0:T(8,128)(2,1)S(1)}, u32[]{:S(2)}, u32[]{:S(2)}) collective-permute-start(bf16[192,2048]{1,0:T(8,128)(2,1)} %get-tuple-element.16), channel_id=1, source_target_pairs={{0,1},{1,0},{2,3},{3,2},{4,7},{5,6},{6,5},{7,4},{8,9},{9,8},{10,11... | collective-permute-start | bytes 2359304 | tf_op jit(solution)/shard_map/ppermute | solution.py:71
  17.4 9.2 %collective-permute-start.6 = (bf16[32,2048]{1,0:T(8,128)(2,1)S(1)}, bf16[32,2048]{1,0:T(8,128)(2,1)S(1)}, u32[]{:S(2)}, u32[]{:S(2)}) collective-permute-start(bf16[32,2048]{1,0:T(8,128)(2,1)S(1)} %copy-done.1), channel_id=1, source_target_pairs={{0,24},{4,12},{8,16},{12,4},{16,8},{20,28},{24,0},{28,20},{32,56},... | collective-permute-start | bytes 393224 | tf_op jit(solution)/shard_map/ppermute | solution.py:58
  18.7 9.0 %collective-permute-start.24 = (bf16[32,2048]{1,0:T(8,128)(2,1)S(1)}, bf16[32,2048]{1,0:T(8,128)(2,1)S(1)}, u32[]{:S(2)}, u32[]{:S(2)}) collective-permute-start(bf16[32,2048]{1,0:T(8,128)(2,1)S(1)} %bitcast.14), channel_id=1, source_target_pairs={{0,224},{4,36},{8,232},{12,44},{16,240},{20,52},{24,248},{28,60},{... | collective-permute-start | bytes 393224 | tf_op jit(solution)/shard_map/ppermute | solution.py:50
  20.3 8.3 %collective-permute-start.23 = (bf16[32,2048]{1,0:T(8,128)(2,1)S(1)}, bf16[32,2048]{1,0:T(8,128)(2,1)S(1)}, u32[]{:S(2)}, u32[]{:S(2)}) collective-permute-start(bf16[32,2048]{1,0:T(8,128)(2,1)S(1)} %bitcast.15), channel_id=1, source_target_pairs={{0,32},{4,228},{8,40},{12,236},{16,48},{20,244},{24,56},{28,252},{... | collective-permute-start | bytes 393224 | tf_op jit(solution)/shard_map/ppermute | solution.py:50
  25.0 5.0 %collective-permute-start.5 = (bf16[32,2048]{1,0:T(8,128)(2,1)S(1)}, bf16[32,2048]{1,0:T(8,128)(2,1)S(1)}, u32[]{:S(2)}, u32[]{:S(2)}) collective-permute-start(bf16[32,2048]{1,0:T(8,128)(2,1)S(1)} %copy-done.1), channel_id=1, source_target_pairs={{0,8},{4,28},{8,0},{12,20},{16,24},{20,12},{24,16},{28,4},{32,40},... | collective-permute-start | bytes 393224 | tf_op jit(solution)/shard_map/ppermute | solution.py:58
  26.6 5.0 %collective-permute-start.7 = (bf16[32,2048]{1,0:T(8,128)(2,1)S(1)}, bf16[32,2048]{1,0:T(8,128)(2,1)S(1)}, u32[]{:S(2)}, u32[]{:S(2)}) collective-permute-start(bf16[32,2048]{1,0:T(8,128)(2,1)S(1)} %collective-permute-done.6.refs_2_), channel_id=1, source_target_pairs={{0,8},{4,28},{8,0},{12,20},{16,24},{20,12},{24,16},{28,4},{32,40},... | collective-permute-start | bytes 393224 | tf_op jit(solution)/shard_map/ppermute | solution.py:58
  27.7 5.0 %collective-permute-start.25 = (bf16[32,2048]{1,0:T(8,128)(2,1)S(1)}, bf16[32,2048]{1,0:T(8,128)(2,1)S(1)}, u32[]{:S(2)}, u32[]{:S(2)}) collective-permute-start(bf16[32,2048]{1,0:T(8,128)(2,1)S(1)} %collective-permute-done.24.refs_4_), channel_id=1, source_target_pairs={{0,32},{4,228},{8,40},{12,236},{16,48},{20,244},{24,56},{28,252},{... | collective-permute-start | bytes 393224 | tf_op jit(solution)/shard_map/ppermute | solution.py:50
  28.6 25.9 %copy-start.5 = (f32[2,2048]{1,0:T(2,128)S(1)}, f32[2,2048]{1,0:T(2,128)}, u32[]{:S(2)}) copy-start(f32[2,2048]{1,0:T(2,128)} %param.18) | copy-start | bytes 49156
  28.6 31.1 %collective-permute-start.1 = (bf16[192,2048]{1,0:T(8,128)(2,1)}, bf16[192,2048]{1,0:T(8,128)(2,1)S(1)}, u32[]{:S(2)}, u32[]{:S(2)}) collective-permute-start(bf16[192,2048]{1,0:T(8,128)(2,1)} %get-tuple-element.14), channel_id=1, source_target_pairs={{0,1},{1,0},{2,3},{3,2},{4,7},{5,6},{6,5},{7,4},{8,9},{9,8},{10,11... | collective-permute-start | bytes 2359304 | tf_op jit(solution)/shard_map/ppermute | solution.py:71
  30.0 5.4 %collective-permute-start.26 = (bf16[32,2048]{1,0:T(8,128)(2,1)S(1)}, bf16[32,2048]{1,0:T(8,128)(2,1)S(1)}, u32[]{:S(2)}, u32[]{:S(2)}) collective-permute-start(bf16[32,2048]{1,0:T(8,128)(2,1)S(1)} %collective-permute-done.23.refs_1_), channel_id=1, source_target_pairs={{0,224},{4,36},{8,232},{12,44},{16,240},{20,52},{24,248},{28,60},{... | collective-permute-start | bytes 393224 | tf_op jit(solution)/shard_map/ppermute | solution.py:50
  32.2 19.5 %collective-permute-start.9 = (bf16[4,32,2048]{2,1,0:T(8,128)(2,1)S(1)}, bf16[4,32,2048]{2,1,0:T(8,128)(2,1)S(1)}, u32[]{:S(2)}, u32[]{:S(2)}) collective-permute-start(bf16[4,32,2048]{2,1,0:T(8,128)(2,1)S(1)} %shard_map.101.refs_2_), channel_id=1, source_target_pairs={{0,224},{4,36},{8,232},{12,44},{16,240},{20,52},{24,248},{28,60},{... | collective-permute-start | bytes 1572872 | tf_op jit(solution)/shard_map/ppermute | solution.py:50
  32.7 9.7 %collective-permute-start.28 = (bf16[32,2048]{1,0:T(8,128)(2,1)S(1)}, bf16[32,2048]{1,0:T(8,128)(2,1)S(1)}, u32[]{:S(2)}, u32[]{:S(2)}) collective-permute-start(bf16[32,2048]{1,0:T(8,128)(2,1)S(1)} %collective-permute-done.25.refs_2_), channel_id=1, source_target_pairs={{0,224},{4,36},{8,232},{12,44},{16,240},{20,52},{24,248},{28,60},{... | collective-permute-start | bytes 393224 | tf_op jit(solution)/shard_map/ppermute | solution.py:50
  34.1 31.3 %copy-start.6 = (f32[2,2048]{1,0:T(2,128)S(1)}, f32[2,2048]{1,0:T(2,128)}, u32[]{:S(2)}) copy-start(f32[2,2048]{1,0:T(2,128)} %param.19) | copy-start | bytes 49156
  34.1 31.3 %copy-start.2 = (bf16[192,2048]{1,0:T(8,128)(2,1)S(1)}, bf16[192,2048]{1,0:T(8,128)(2,1)}, u32[]{:S(2)}) copy-start(bf16[192,2048]{1,0:T(8,128)(2,1)} %param.13) | copy-start | bytes 2359300
  34.1 31.3 %copy-start.3 = (bf16[192,2048]{1,0:T(8,128)(2,1)S(1)}, bf16[192,2048]{1,0:T(8,128)(2,1)}, u32[]{:S(2)}) copy-start(bf16[192,2048]{1,0:T(8,128)(2,1)} %get-tuple-element.13) | copy-start | bytes 2359300
  34.1 28.3 %collective-permute-start.3 = (bf16[192,2048]{1,0:T(8,128)(2,1)S(1)}, bf16[192,2048]{1,0:T(8,128)(2,1)S(1)}, u32[]{:S(2)}, u32[]{:S(2)}) collective-permute-start(bf16[192,2048]{1,0:T(8,128)(2,1)S(1)} %add_convert_fusion.3), channel_id=1, source_target_pairs={{0,3},{1,2},{2,1},{3,0},{4,5},{5,4},{6,7},{7,6},{8,11},{9,10},{10,... | collective-permute-start | bytes 2359304 | tf_op jit(solution)/shard_map/ppermute | solution.py:71
  35.4 9.0 %collective-permute-start.27 = (bf16[32,2048]{1,0:T(8,128)(2,1)S(1)}, bf16[32,2048]{1,0:T(8,128)(2,1)S(1)}, u32[]{:S(2)}, u32[]{:S(2)}) collective-permute-start(bf16[32,2048]{1,0:T(8,128)(2,1)S(1)} %collective-permute-done.26.refs_5_), channel_id=1, source_target_pairs={{0,32},{4,228},{8,40},{12,236},{16,48},{20,244},{24,56},{28,252},{... | collective-permute-start | bytes 393224 | tf_op jit(solution)/shard_map/ppermute | solution.py:50
  42.5 7.1 %collective-permute-start.29 = (bf16[32,2048]{1,0:T(8,128)(2,1)S(1)}, bf16[32,2048]{1,0:T(8,128)(2,1)S(1)}, u32[]{:S(2)}, u32[]{:S(2)}) collective-permute-start(bf16[32,2048]{1,0:T(8,128)(2,1)S(1)} %collective-permute-done.28.refs_6_), channel_id=1, source_target_pairs={{0,32},{4,228},{8,40},{12,236},{16,48},{20,244},{24,56},{28,252},{... | collective-permute-start | bytes 393224 | tf_op jit(solution)/shard_map/ppermute | solution.py:50
  44.5 10.7 %collective-permute-start.15 = (bf16[4,32,2048]{2,1,0:T(8,128)(2,1)S(1)}, bf16[4,32,2048]{2,1,0:T(8,128)(2,1)S(1)}, u32[]{:S(2)}, u32[]{:S(2)}) collective-permute-start(bf16[4,32,2048]{2,1,0:T(8,128)(2,1)S(1)} %shard_map.101.refs_2_), channel_id=1, source_target_pairs={{0,4},{4,0},{8,12},{12,8},{16,20},{20,16},{24,28},{28,24},{32,36},... | collective-permute-start | bytes 1572872 | tf_op jit(solution)/shard_map/ppermute | solution.py:79
  49.6 9.2 %collective-permute-start.8 = (bf16[4,32,2048]{2,1,0:T(8,128)(2,1)S(1)}, bf16[4,32,2048]{2,1,0:T(8,128)(2,1)S(1)}, u32[]{:S(2)}, u32[]{:S(2)}) collective-permute-start(bf16[4,32,2048]{2,1,0:T(8,128)(2,1)S(1)} %shard_map.101.refs_2_), channel_id=1, source_target_pairs={{0,32},{4,228},{8,40},{12,236},{16,48},{20,244},{24,56},{28,252},{... | collective-permute-start | bytes 1572872 | tf_op jit(solution)/shard_map/ppermute | solution.py:50
  51.7 8.3 %collective-permute-start.19 = (bf16[4,32,2048]{2,1,0:T(8,128)(2,1)S(1)}, bf16[4,32,2048]{2,1,0:T(8,128)(2,1)S(1)}, u32[]{:S(2)}, u32[]{:S(2)}) collective-permute-start(bf16[4,32,2048]{2,1,0:T(8,128)(2,1)S(1)} %collective-permute-done.9.refs_6_), channel_id=1, source_target_pairs={{0,4},{4,0},{8,12},{12,8},{16,20},{20,16},{24,28},{28,24},{32,36},... | collective-permute-start | bytes 1572872 | tf_op jit(solution)/shard_map/ppermute | solution.py:79
  55.2 31.4 %collective-permute-start.33 = (bf16[8,32,2048]{2,1,0:T(8,128)(2,1)S(1)}, bf16[8,32,2048]{2,1,0:T(8,128)(2,1)S(1)}, u32[]{:S(2)}, u32[]{:S(2)}) collective-permute-start(bf16[8,32,2048]{2,1,0:T(8,128)(2,1)S(1)} %shard_map.102.refs_18_), channel_id=1, source_target_pairs={{0,4},{4,0},{8,12},{12,8},{16,20},{20,16},{24,28},{28,24},{32,36},... | collective-permute-start | bytes 3145736 | tf_op jit(solution)/shard_map/ppermute | solution.py:79
  58.8 27.8 %collective-permute-start.31 = (bf16[8,32,2048]{2,1,0:T(8,128)(2,1)S(1)}, bf16[8,32,2048]{2,1,0:T(8,128)(2,1)S(1)}, u32[]{:S(2)}, u32[]{:S(2)}) collective-permute-start(bf16[8,32,2048]{2,1,0:T(8,128)(2,1)S(1)} %shard_map.102.refs_18_), channel_id=1, source_target_pairs={{0,24},{4,12},{8,16},{12,4},{16,8},{20,28},{24,0},{28,20},{32,56},... | collective-permute-start | bytes 3145736 | tf_op jit(solution)/shard_map/ppermute | solution.py:58
  59.7 27.1 %collective-permute-start.30 = (bf16[8,32,2048]{2,1,0:T(8,128)(2,1)S(1)}, bf16[8,32,2048]{2,1,0:T(8,128)(2,1)S(1)}, u32[]{:S(2)}, u32[]{:S(2)}) collective-permute-start(bf16[8,32,2048]{2,1,0:T(8,128)(2,1)S(1)} %shard_map.102.refs_18_), channel_id=1, source_target_pairs={{0,8},{4,28},{8,0},{12,20},{16,24},{20,12},{24,16},{28,4},{32,40},... | collective-permute-start | bytes 3145736 | tf_op jit(solution)/shard_map/ppermute | solution.py:58
  60.0 9.5 %collective-permute-start.10 = (bf16[4,32,2048]{2,1,0:T(8,128)(2,1)S(1)}, bf16[4,32,2048]{2,1,0:T(8,128)(2,1)S(1)}, u32[]{:S(2)}, u32[]{:S(2)}) collective-permute-start(bf16[4,32,2048]{2,1,0:T(8,128)(2,1)S(1)} %collective-permute-done.9.refs_6_), channel_id=1, source_target_pairs={{0,32},{4,228},{8,40},{12,236},{16,48},{20,244},{24,56},{28,252},{... | collective-permute-start | bytes 1572872 | tf_op jit(solution)/shard_map/ppermute | solution.py:50
  62.4 7.1 %collective-permute-start.16 = (bf16[4,32,2048]{2,1,0:T(8,128)(2,1)S(1)}, bf16[4,32,2048]{2,1,0:T(8,128)(2,1)S(1)}, u32[]{:S(2)}, u32[]{:S(2)}) collective-permute-start(bf16[4,32,2048]{2,1,0:T(8,128)(2,1)S(1)} %collective-permute-done.8.refs_3_), channel_id=1, source_target_pairs={{0,4},{4,0},{8,12},{12,8},{16,20},{20,16},{24,28},{28,24},{32,36},... | collective-permute-start | bytes 1572872 | tf_op jit(solution)/shard_map/ppermute | solution.py:79
  69.6 10.1 %collective-permute-start.11 = (bf16[4,32,2048]{2,1,0:T(8,128)(2,1)S(1)}, bf16[4,32,2048]{2,1,0:T(8,128)(2,1)S(1)}, u32[]{:S(2)}, u32[]{:S(2)}) collective-permute-start(bf16[4,32,2048]{2,1,0:T(8,128)(2,1)S(1)} %collective-permute-done.8.refs_3_), channel_id=1, source_target_pairs={{0,224},{4,36},{8,232},{12,44},{16,240},{20,52},{24,248},{28,60},{... | collective-permute-start | bytes 1572872 | tf_op jit(solution)/shard_map/ppermute | solution.py:50
  69.6 20.7 %collective-permute-start.13 = (bf16[4,32,2048]{2,1,0:T(8,128)(2,1)S(1)}, bf16[4,32,2048]{2,1,0:T(8,128)(2,1)S(1)}, u32[]{:S(2)}, u32[]{:S(2)}) collective-permute-start(bf16[4,32,2048]{2,1,0:T(8,128)(2,1)S(1)} %collective-permute-done.10.refs_4_), channel_id=1, source_target_pairs={{0,224},{4,36},{8,232},{12,44},{16,240},{20,52},{24,248},{28,60},{... | collective-permute-start | bytes 1572872 | tf_op jit(solution)/shard_map/ppermute | solution.py:50
  79.7 14.6 %collective-permute-start.17 = (bf16[4,32,2048]{2,1,0:T(8,128)(2,1)S(1)}, bf16[4,32,2048]{2,1,0:T(8,128)(2,1)S(1)}, u32[]{:S(2)}, u32[]{:S(2)}) collective-permute-start(bf16[4,32,2048]{2,1,0:T(8,128)(2,1)S(1)} %collective-permute-done.10.refs_4_), channel_id=1, source_target_pairs={{0,4},{4,0},{8,12},{12,8},{16,20},{20,16},{24,28},{28,24},{32,36},... | collective-permute-start | bytes 1572872 | tf_op jit(solution)/shard_map/ppermute | solution.py:79
  86.7 10.5 %collective-permute-start.20 = (bf16[4,32,2048]{2,1,0:T(8,128)(2,1)S(1)}, bf16[4,32,2048]{2,1,0:T(8,128)(2,1)S(1)}, u32[]{:S(2)}, u32[]{:S(2)}) collective-permute-start(bf16[4,32,2048]{2,1,0:T(8,128)(2,1)S(1)} %collective-permute-done.11.refs_7_), channel_id=1, source_target_pairs={{0,4},{4,0},{8,12},{12,8},{16,20},{20,16},{24,28},{28,24},{32,36},... | collective-permute-start | bytes 1572872 | tf_op jit(solution)/shard_map/ppermute | solution.py:79
  86.7 10.5 %collective-permute-start.12 = (bf16[4,32,2048]{2,1,0:T(8,128)(2,1)S(1)}, bf16[4,32,2048]{2,1,0:T(8,128)(2,1)S(1)}, u32[]{:S(2)}, u32[]{:S(2)}) collective-permute-start(bf16[4,32,2048]{2,1,0:T(8,128)(2,1)S(1)} %collective-permute-done.11.refs_7_), channel_id=1, source_target_pairs={{0,32},{4,228},{8,40},{12,236},{16,48},{20,244},{24,56},{28,252},{... | collective-permute-start | bytes 1572872 | tf_op jit(solution)/shard_map/ppermute | solution.py:50
  86.8 17.6 %collective-permute-start.32 = (bf16[8,32,2048]{2,1,0:T(8,128)(2,1)S(1)}, bf16[8,32,2048]{2,1,0:T(8,128)(2,1)S(1)}, u32[]{:S(2)}, u32[]{:S(2)}) collective-permute-start(bf16[8,32,2048]{2,1,0:T(8,128)(2,1)S(1)} %collective-permute-done.31.refs_20_), channel_id=1, source_target_pairs={{0,8},{4,28},{8,0},{12,20},{16,24},{20,12},{24,16},{28,4},{32,40},... | collective-permute-start | bytes 3145736 | tf_op jit(solution)/shard_map/ppermute | solution.py:58
  90.2 7.5 %collective-permute-start.21 = (bf16[4,32,2048]{2,1,0:T(8,128)(2,1)S(1)}, bf16[4,32,2048]{2,1,0:T(8,128)(2,1)S(1)}, u32[]{:S(2)}, u32[]{:S(2)}) collective-permute-start(bf16[4,32,2048]{2,1,0:T(8,128)(2,1)S(1)} %collective-permute-done.13.refs_8_), channel_id=1, source_target_pairs={{0,4},{4,0},{8,12},{12,8},{16,20},{20,16},{24,28},{28,24},{32,36},... | collective-permute-start | bytes 1572872 | tf_op jit(solution)/shard_map/ppermute | solution.py:79
  94.3 9.6 %collective-permute-start.14 = (bf16[4,32,2048]{2,1,0:T(8,128)(2,1)S(1)}, bf16[4,32,2048]{2,1,0:T(8,128)(2,1)S(1)}, u32[]{:S(2)}, u32[]{:S(2)}) collective-permute-start(bf16[4,32,2048]{2,1,0:T(8,128)(2,1)S(1)} %collective-permute-done.13.refs_8_), channel_id=1, source_target_pairs={{0,32},{4,228},{8,40},{12,236},{16,48},{20,244},{24,56},{28,252},{... | collective-permute-start | bytes 1572872 | tf_op jit(solution)/shard_map/ppermute | solution.py:50
  97.2 6.7 %collective-permute-start.18 = (bf16[4,32,2048]{2,1,0:T(8,128)(2,1)S(1)}, bf16[4,32,2048]{2,1,0:T(8,128)(2,1)S(1)}, u32[]{:S(2)}, u32[]{:S(2)}) collective-permute-start(bf16[4,32,2048]{2,1,0:T(8,128)(2,1)S(1)} %collective-permute-done.12.refs_5_), channel_id=1, source_target_pairs={{0,4},{4,0},{8,12},{12,8},{16,20},{20,16},{24,28},{28,24},{32,36},... | collective-permute-start | bytes 1572872 | tf_op jit(solution)/shard_map/ppermute | solution.py:79
  97.2 16.3 %collective-permute-start.4 = (bf16[192,2048]{1,0:T(8,128)(2,1)S(1)}, bf16[192,2048]{1,0:T(8,128)(2,1)S(1)}, u32[]{:S(2)}, u32[]{:S(2)}) collective-permute-start(bf16[192,2048]{1,0:T(8,128)(2,1)S(1)} %add_convert_fusion.2.refs_1_), channel_id=1, source_target_pairs={{0,3},{1,2},{2,1},{3,0},{4,5},{5,4},{6,7},{7,6},{8,11},{9,10},{10,... | collective-permute-start | bytes 2359304 | tf_op jit(solution)/shard_map/ppermute | solution.py:71
  97.8 20.4 %collective-permute-start.38 = (bf16[192,2048]{1,0:T(8,128)(2,1)S(1)}, bf16[192,2048]{1,0:T(8,128)(2,1)S(1)}, u32[]{:S(2)}, u32[]{:S(2)}) collective-permute-start(bf16[192,2048]{1,0:T(8,128)(2,1)S(1)} %add_convert_fusion.2.refs_1_), channel_id=1, source_target_pairs={{0,1},{1,0},{2,3},{3,2},{4,7},{5,6},{6,5},{7,4},{8,9},{9,8},{10,11... | collective-permute-start | bytes 2359304 | tf_op jit(solution)/shard_map/ppermute | solution.py:71
  103.9 15.5 %collective-permute-start.35 = (bf16[8,32,2048]{2,1,0:T(8,128)(2,1)S(1)}, bf16[8,32,2048]{2,1,0:T(8,128)(2,1)S(1)}, u32[]{:S(2)}, u32[]{:S(2)}) collective-permute-start(bf16[8,32,2048]{2,1,0:T(8,128)(2,1)S(1)} %collective-permute-done.31.refs_20_), channel_id=1, source_target_pairs={{0,4},{4,0},{8,12},{12,8},{16,20},{20,16},{24,28},{28,24},{32,36},... | collective-permute-start | bytes 3145736 | tf_op jit(solution)/shard_map/ppermute | solution.py:79
  103.9 15.5 %collective-permute-start.34 = (bf16[8,32,2048]{2,1,0:T(8,128)(2,1)S(1)}, bf16[8,32,2048]{2,1,0:T(8,128)(2,1)S(1)}, u32[]{:S(2)}, u32[]{:S(2)}) collective-permute-start(bf16[8,32,2048]{2,1,0:T(8,128)(2,1)S(1)} %collective-permute-done.30.refs_19_), channel_id=1, source_target_pairs={{0,4},{4,0},{8,12},{12,8},{16,20},{20,16},{24,28},{28,24},{32,36},... | collective-permute-start | bytes 3145736 | tf_op jit(solution)/shard_map/ppermute | solution.py:79
  104.4 22.3 %collective-permute-start.36 = (bf16[8,32,2048]{2,1,0:T(8,128)(2,1)S(1)}, bf16[8,32,2048]{2,1,0:T(8,128)(2,1)S(1)}, u32[]{:S(2)}, u32[]{:S(2)}) collective-permute-start(bf16[8,32,2048]{2,1,0:T(8,128)(2,1)S(1)} %collective-permute-done.32.refs_21_), channel_id=1, source_target_pairs={{0,4},{4,0},{8,12},{12,8},{16,20},{20,16},{24,28},{28,24},{32,36},... | collective-permute-start | bytes 3145736 | tf_op jit(solution)/shard_map/ppermute | solution.py:79
  113.6 13.1 %collective-permute-start.37 = (bf16[192,2048]{1,0:T(8,128)(2,1)S(1)}, bf16[192,2048]{1,0:T(8,128)(2,1)S(1)}, u32[]{:S(2)}, u32[]{:S(2)}) collective-permute-start(bf16[192,2048]{1,0:T(8,128)(2,1)S(1)} %collective-permute-done.4.refs_0_), channel_id=1, source_target_pairs={{0,1},{1,0},{2,3},{3,2},{4,7},{5,6},{6,5},{7,4},{8,9},{9,8},{10,11... | collective-permute-start | bytes 2359304 | tf_op jit(solution)/shard_map/ppermute | solution.py:71
  118.1 2.7 %collective-permute-start.22 = (bf16[4,32,2048]{2,1,0:T(8,128)(2,1)S(1)}, bf16[4,32,2048]{2,1,0:T(8,128)(2,1)S(1)}, u32[]{:S(2)}, u32[]{:S(2)}) collective-permute-start(bf16[4,32,2048]{2,1,0:T(8,128)(2,1)S(1)} %collective-permute-done.14.refs_9_), channel_id=1, source_target_pairs={{0,4},{4,0},{8,12},{12,8},{16,20},{20,16},{24,28},{28,24},{32,36},... | collective-permute-start | bytes 1572872 | tf_op jit(solution)/shard_map/ppermute | solution.py:79
  136.7 12.8 %collective-permute-start.40 = (bf16[192,2048]{1,0:T(8,128)(2,1)S(1)}, bf16[192,2048]{1,0:T(8,128)(2,1)S(1)}, u32[]{:S(2)}, u32[]{:S(2)}) collective-permute-start(bf16[192,2048]{1,0:T(8,128)(2,1)S(1)} %get-tuple-element.20), channel_id=1, source_target_pairs={{0,1},{1,0},{2,3},{3,2},{4,7},{5,6},{6,5},{7,4},{8,9},{9,8},{10,11... | collective-permute-start | bytes 2359304 | tf_op jit(solution)/shard_map/ppermute | solution.py:71
  139.0 18.3 %collective-permute-start.39 = (bf16[192,2048]{1,0:T(8,128)(2,1)S(1)}, bf16[192,2048]{1,0:T(8,128)(2,1)S(1)}, u32[]{:S(2)}, u32[]{:S(2)}) collective-permute-start(bf16[192,2048]{1,0:T(8,128)(2,1)S(1)} %get-tuple-element.18), channel_id=1, source_target_pairs={{0,1},{1,0},{2,3},{3,2},{4,7},{5,6},{6,5},{7,4},{8,9},{9,8},{10,11... | collective-permute-start | bytes 2359304 | tf_op jit(solution)/shard_map/ppermute | solution.py:71
  149.8 19.6 %collective-permute-start.41 = (bf16[192,2048]{1,0:T(8,128)(2,1)S(1)}, bf16[192,2048]{1,0:T(8,128)(2,1)S(1)}, u32[]{:S(2)}, u32[]{:S(2)}) collective-permute-start(bf16[192,2048]{1,0:T(8,128)(2,1)S(1)} %add_convert_fusion.1), channel_id=1, source_target_pairs={{0,3},{1,2},{2,1},{3,0},{4,5},{5,4},{6,7},{7,6},{8,11},{9,10},{10,... | collective-permute-start | bytes 2359304 | tf_op jit(solution)/shard_map/ppermute | solution.py:71
